TPU v7x, 32 devices: a whole 2x2x4 slice. The times are simulated.
32 devices in a mesh: rep: 2 (over x), fs: 8 (over z, y), tp: 2 (over core).
Axes of the slice: x: 2, y: 2, z: 4, core: 2. Of those that a mesh axis runs over, the one named last changes fastest.
Arguments:
- inputs: bfloat16 [8192, 2048], P(('rep', 'fs')), may hold values from -6 to 6
- cotangent: bfloat16 [8192, 2048], P(('rep', 'fs')), may hold values from -6 to 6
- gate_weight: bfloat16 [2048, 4096], P('fs', 'tp'), may hold values from -0.125 to 0.125
- up_weight: bfloat16 [2048, 4096], P('fs', 'tp'), may hold values from -0.125 to 0.125
- down_weight: bfloat16 [2048, 4096], P('fs', 'tp'), may hold values from -0.09375 to 0.09375
Outputs:
- grad_input: bfloat16 [8192, 2048], P(('rep', 'fs'))
- grad_down: float32 [2048, 4096], P('fs', 'tp')
All inputs are finite; a program needn't handle non-finite values.
Results may differ from a plain program's by a relative error of at most 0.014.
Values may be sent and summed in bfloat16 or wider, within the bound.
A program may use at most 128 MiB of HBM per device.

v0:
```python
import functools
import math

import jax
import jax.numpy as jnp
from jax import lax
from jax.experimental import pallas as pl
from jax.experimental.pallas import tpu as pltpu
from jax.sharding import PartitionSpec as P

MESH = pl.DeviceIdType.MESH


def gather_kernel(
    line, units, gate_w, up_w, down_w, toks, cots, gu_out, d_out, t_out, w_tmp, t_tmp,
    up_s, up_r, dn_s, dn_r, y_s, y_r, tok_s, tok_r, d2d_s, d2d_r, loc, loc2,
):
    r = lax.axis_index("rep")
    f = lax.axis_index("fs")
    t = lax.axis_index("tp")
    z, y = f // 2, f % 2
    rows = toks.shape[0]
    half = rows // 2
    wrows = gate_w.shape[0]
    width = gate_w.shape[1] // 4
    parts = len(units)
    has_up, has_dn = z < line - 1, z > 0
    up = {"fs": (f + 2) % (2 * line)}
    dn = {"fs": (f + 2 * line - 2) % (2 * line)}
    ypart = {"fs": f + 1 - 2 * y}
    xpart = {"rep": 1 - r}
    core = t % 2
    cpart = {"tp": t + 1 - 2 * core}

    barrier = pltpu.get_barrier_semaphore()

    def greet(dev):
        pl.semaphore_signal(barrier, inc=1, device_id=dev, device_id_type=MESH)

    for dev in (ypart, xpart, cpart, up, dn):
        greet(dev)
    pl.semaphore_wait(barrier, 5)

    def remote(src, dst, s, q, dev):
        return pltpu.make_async_remote_copy(
            src_ref=src, dst_ref=dst, send_sem=s, recv_sem=q,
            device_id=dev, device_id_type=MESH,
        )

    def wblk(k, zz, yy):
        row = pl.multiple_of((2 * zz + yy) * wrows, wrows)
        which, col, wide = units[k]
        return (gu_out, d_out)[which].at[pl.ds(row, wrows), pl.ds(col, wide)]

    def own(k, yy):
        col = pl.multiple_of((2 * r + yy) * width, width)
        return (gate_w, up_w, down_w)[k].at[:, pl.ds(col, width)]

    def to_y(k):
        return remote(own(k, 1 - y), wblk(k, z, y), y_s.at[k], y_r.at[k], ypart)

    def from_y(k):
        return remote(own(k, 1 - y), wblk(k, z, 1 - y), y_s.at[k], y_r.at[k], ypart)

    def zcopy(up_dir, d, sub, k, zz):
        yy = y if sub == 0 else 1 - y
        src = own(k, y) if (d == 0 and sub == 0) else wblk(k, zz, yy)
        s, q, dev = (up_s, up_r, up) if up_dir else (dn_s, dn_r, dn)
        return remote(src, wblk(k, zz, yy), s.at[d, sub, k], q.at[d, sub, k], dev)

    def pred_send(up_dir, d):
        return (has_up & (z - d >= 0)) if up_dir else (has_dn & (z + d <= line - 1))

    def src_z(up_dir, d):
        return jnp.maximum(z - d, 0) if up_dir else jnp.minimum(z + d, line - 1)

    def send(up_dir, d, sub, k):
        @pl.when(pred_send(up_dir, d))
        def _():
            zcopy(up_dir, d, sub, k, src_z(up_dir, d)).start()

    def await_send(up_dir, d, sub, k):
        @pl.when(pred_send(up_dir, d))
        def _():
            zcopy(up_dir, d, sub, k, src_z(up_dir, d)).wait_send()

    def await_recv(up_dir, d, sub, k):
        ok = (z - d - 1 >= 0) if up_dir else (z + d + 1 <= line - 1)

        @pl.when(ok)
        def _():
            zcopy(up_dir, d, sub, k, src_z(up_dir, d + 1)).wait_recv()

    def tblk(j, rr, yy, c):
        row = pl.multiple_of((2 * rr + yy) * rows + c * half, half)
        return t_out.at[j, pl.ds(row, half), :]

    def mine(j):
        src = toks if j == 0 else cots
        return src.at[pl.ds(pl.multiple_of(core * half, half), half), :]

    def tcopy(i, landing):
        j = (0, 1, 0, 1, 0, 1)[i]
        dev = xpart if i in (0, 1, 5) else ypart
        if landing:
            rr = (1 - r, 1 - r, r, r, 1 - r, 1 - r)[i]
            yy = (y, y, 1 - y, 1 - y, 1 - y, 1 - y)[i]
            src = dst = tblk(j, rr, yy, core)
        else:
            rr = (r, r, r, r, 1 - r, r)[i]
            yy = (y, y, y, y, y, 1 - y)[i]
            dst = tblk(j, rr, yy, core)
            src = mine(j) if i < 4 else dst
        return remote(src, dst, tok_s.at[i], tok_r.at[i], dev)

    def dcopy(i, c):
        j = (0, 1, 0, 1, 0, 1)[i]
        rr = (1 - r, 1 - r, r, r, 1 - r, 1 - r)[i]
        yy = (y, y, 1 - y, 1 - y, 1 - y, 1 - y)[i]
        blk = tblk(j, rr, yy, c)
        return remote(blk, blk, d2d_s.at[i], d2d_r.at[i], cpart)

    loads = [
        pltpu.make_async_copy(own(0, y), w_tmp.at[0], loc.at[0]),
        pltpu.make_async_copy(own(1, y), w_tmp.at[1], loc.at[3]),
        pltpu.make_async_copy(own(2, y), w_tmp.at[2], loc.at[4]),
        pltpu.make_async_copy(toks, t_tmp.at[0], loc.at[1]),
        pltpu.make_async_copy(cots, t_tmp.at[1], loc.at[2]),
    ]
    trow = pl.multiple_of((2 * r + y) * rows, rows)
    stores = [
        pltpu.make_async_copy(w_tmp.at[0], wblk(0, z, y), loc2.at[0]),
        pltpu.make_async_copy(w_tmp.at[1], wblk(1, z, y), loc2.at[3]),
        pltpu.make_async_copy(w_tmp.at[2], wblk(2, z, y), loc2.at[4]),
        pltpu.make_async_copy(t_tmp.at[0], t_out.at[0, pl.ds(trow, rows), :], loc2.at[1]),
        pltpu.make_async_copy(t_tmp.at[1], t_out.at[1, pl.ds(trow, rows), :], loc2.at[2]),
    ]

    for k in range(parts):
        to_y(k).start()
        send(True, 0, 0, k)
        send(False, 0, 0, k)
    for i in (0, 1, 3, 2):
        tcopy(i, False).start()
    for copy in loads:
        copy.start()
    for load, store in zip(loads, stores):
        load.wait()
        store.start()
    for k in range(parts):
        from_y(k).wait_recv()
        send(True, 0, 1, k)
        send(False, 0, 1, k)

    def event(i):
        tcopy(i, True).wait_recv()
        if i == 0:
            tcopy(4, False).start()
        if i == 3:
            tcopy(5, False).start()
        dcopy(i, core).start()

    events = [0, 3, 1, 2, 5, 4]
    for d in range(line - 1):
        for sub in range(2):
            if events:
                event(events.pop(0))
            for k in range(parts):
                for up_dir in (True, False):
                    await_recv(up_dir, d, sub, k)
                    if d + 1 < line - 1:
                        send(up_dir, d + 1, sub, k)
    for i in events:
        event(i)
    for i in range(6):
        dcopy(i, 1 - core).wait_recv()
        dcopy(i, core).wait_send()
        tcopy(i, False).wait_send()
    for k in range(parts):
        to_y(k).wait_send()
        for d in range(line - 1):
            for sub in range(2):
                await_send(True, d, sub, k)
                await_send(False, d, sub, k)
    for store in stores:
        store.wait()


def gather(gate_w, up_w, down_w, toks, cots):
    line = lax.axis_size("fs") // 2
    wrows, width = gate_w.shape[0], gate_w.shape[1] // 4
    units = [(0, 0, width), (0, width, width), (1, 0, width)]
    parts = len(units)
    depth = 2 * line * wrows
    kind = gate_w.dtype
    dma = pltpu.SemaphoreType.DMA
    zsem = dma((line - 1, 2, parts))
    anyspec = pl.BlockSpec(memory_space=pl.ANY)
    return pl.pallas_call(
        functools.partial(gather_kernel, line, units),
        out_shape=(
            jax.ShapeDtypeStruct((depth, 2 * width), kind),
            jax.ShapeDtypeStruct((depth, width), kind),
            jax.ShapeDtypeStruct((2, 4 * toks.shape[0], toks.shape[1]), toks.dtype),
        ),
        in_specs=[anyspec] * 5,
        out_specs=(anyspec,) * 3,
        scratch_shapes=[
            pltpu.VMEM((parts, wrows, width), kind),
            pltpu.VMEM((2,) + toks.shape, toks.dtype),
            zsem, zsem, zsem, zsem,
            dma((parts,)), dma((parts,)),
            dma((6,)), dma((6,)), dma((6,)), dma((6,)),
            dma((5,)), dma((5,)),
        ],
        compiler_params=pltpu.CompilerParams(collective_id=0, has_side_effects=True),
        name="gather_all",
    )(gate_w, up_w, down_w, toks, cots)


def reduce_kernel(
    line, p_in, g_in, gi_out, gd_out,
    p_tmp, r1, s1, rx, ry, s3, fin, u_in, d_in, u_out, d_out, gfin,
    c_s, c_r, x_s, x_r, yy_s, yy_r, u_s, u_r, d_s, d_r, f_s, f_r, o_s, o_r, loc,
):
    r = lax.axis_index("rep")
    f = lax.axis_index("fs")
    core = lax.axis_index("tp")
    z, y = f // 2, f % 2
    rows = p_in.shape[0] // 4
    cols = p_in.shape[1] // 2
    side = cols // 2
    width = g_in.shape[1]
    zrows = g_in.shape[0] // line
    frows = zrows // 2
    up = {"fs": (f + 2) % (2 * line)}
    dn = {"fs": (f + 2 * line - 2) % (2 * line)}
    ypart = {"fs": f + 1 - 2 * y}
    xpart = {"rep": 1 - r}
    cpart = {"tp": 1 - core}

    barrier = pltpu.get_barrier_semaphore()
    for dev in (ypart, xpart, cpart, up, dn):
        pl.semaphore_signal(barrier, inc=1, device_id=dev, device_id_type=MESH)
    pl.semaphore_wait(barrier, 5)

    def remote(src, dst, s, q, dev):
        return pltpu.make_async_remote_copy(
            src_ref=src, dst_ref=dst, send_sem=s, recv_sem=q,
            device_id=dev, device_id_type=MESH,
        )

    def total(dst, terms, count, step=64):
        @pl.loop(0, count // step)
        def _(i):
            at = pl.multiple_of(i * step, step)
            value = None
            for ref, row, col, wide in terms:
                one = ref[pl.ds(row + at, step), pl.ds(col, wide)].astype(jnp.float32)
                value = one if value is None else value + one
            ref, row, col, wide = dst
            ref[pl.ds(row + at, step), pl.ds(col, wide)] = value.astype(ref.dtype)

    def slot(rr, yy):
        return pl.multiple_of((2 * rr + yy) * rows, rows)

    order = [(1 - r, 1 - y), (1 - r, y), (r, 1 - y), (r, y)]
    my_col = pl.multiple_of(core * cols, cols)
    its_col = pl.multiple_of((1 - core) * cols, cols)

    def core_copy(i):
        at = pl.ds(slot(*order[i]), rows)
        return remote(p_in.at[at, pl.ds(its_col, cols)], r1.at[at, :], c_s.at[i], c_r.at[i], cpart)

    def s1_half(i, second):
        return s1.at[pl.ds(slot(*order[i]), rows), pl.ds(side if second else 0, side)]

    def x_copy(i):
        src = (s1_half(0, False), s1_half(1, False), s3.at[1])[i]
        return remote(src, rx.at[i], x_s.at[i], x_r.at[i], xpart)

    def y_copy(i):
        src = (s1_half(0, True), s1_half(2, True), s3.at[0])[i]
        return remote(src, ry.at[i], yy_s.at[i], yy_r.at[i], ypart)

    def block(ref, zt):
        return ref.at[pl.ds(zt * zrows, zrows), :]

    def up_copy(zt, first):
        return remote(block(g_in if first else u_out, zt), block(u_in, zt), u_s.at[zt], u_r.at[zt], up)

    def dn_copy(zt, first):
        return remote(block(g_in if first else d_out, zt), block(d_in, zt), d_s.at[zt], d_r.at[zt], dn)

    def line_step(i):
        zt = line - 1 - i
        if zt > 0:
            @pl.when((z > 0) & (z < zt))
            def _():
                up_copy(zt, False).wait_recv()
                row = zt * zrows
                total((u_out, row, 0, width), [(g_in, row, 0, width), (u_in, row, 0, width)], zrows)
                up_copy(zt, False).start()

            zd = i

            @pl.when((z < line - 1) & (z > zd))
            def _():
                dn_copy(zd, False).wait_recv()
                row = zd * zrows
                total((d_out, row, 0, width), [(g_in, row, 0, width), (d_in, row, 0, width)], zrows)
                dn_copy(zd, False).start()

    def p_load(i):
        at = pl.ds(slot(*order[i]), rows)
        return pltpu.make_async_copy(p_in.at[at, pl.ds(my_col, cols)], p_tmp.at[at, :], loc.at[3 + i])

    for i in range(4):
        core_copy(i).start()
        p_load(i).start()
    for i in range(line - 1):
        @pl.when(z == 0)
        def _():
            up_copy(line - 1 - i, True).start()

        @pl.when(z == line - 1)
        def _():
            dn_copy(i, True).start()

    for i in range(4):
        p_load(i).wait()
        core_copy(i).wait_recv()
        row = slot(*order[i])
        total((s1, row, 0, cols), [(p_tmp, row, 0, cols), (r1, row, 0, cols)], rows)
        if i in (0, 1):
            x_copy(i).start()
        if i == 0:
            y_copy(0).start()
        if i == 2:
            y_copy(1).start()

    line_step(0)
    x_copy(0).wait_recv()
    total((s3.at[0], 0, 0, side), [(s1, slot(r, 1 - y), 0, side), (rx.at[0], 0, 0, side)], rows)
    y_copy(2).start()
    y_copy(0).wait_recv()
    total((s3.at[1], 0, 0, side), [(s1, slot(1 - r, y), side, side), (ry.at[0], 0, 0, side)], rows)
    x_copy(2).start()
    for i in range(1, line - 1):
        line_step(i)

    zrow = pl.multiple_of(z * zrows, zrows)

    def here(ref):
        return (ref, zrow, 0, width)

    @pl.when(z == 0)
    def _():
        dn_copy(0, True).wait_recv()
        total((gfin, 0, 0, width), [here(g_in), here(d_in)], zrows)

    @pl.when(z == line - 1)
    def _():
        up_copy(line - 1, True).wait_recv()
        total((gfin, 0, 0, width), [here(g_in), here(u_in)], zrows)

    @pl.when((z > 0) & (z < line - 1))
    def _():
        remote(block(g_in, z), block(u_in, z), u_s.at[z], u_r.at[z], up).wait_recv()
        remote(block(g_in, z), block(d_in, z), d_s.at[z], d_r.at[z], dn).wait_recv()
        total((gfin, 0, 0, width), [here(g_in), here(u_in), here(d_in)], zrows)

    def gcols(rr, yy):
        return gd_out.at[:, pl.ds(pl.multiple_of((2 * rr + yy) * width, width), width)]

    def grows(yy):
        return gfin.at[pl.ds(pl.multiple_of(yy * frows, frows), frows), :]

    def f_copy(i, landing):
        if i == 0:
            dst = gcols(r, 1 - y) if landing else gcols(r, y)
            return remote(grows(1 - y), dst, f_s.at[0], f_r.at[0], ypart)
        if i == 1:
            dst = gcols(1 - r, y) if landing else gcols(r, y)
            return remote(grows(y), dst, f_s.at[1], f_r.at[1], xpart)
        dst = gcols(1 - r, 1 - y) if landing else gcols(r, 1 - y)
        return remote(gcols(r, 1 - y), dst, f_s.at[2], f_r.at[2], xpart)

    f_copy(0, False).start()
    f_copy(1, False).start()
    own_g = pltpu.make_async_copy(grows(y), gcols(r, y), loc.at[0])
    own_g.start()

    x_copy(1).wait_recv()
    y_copy(2).wait_recv()
    here_row = slot(r, y)
    total(
        (fin, 0, 0, side),
        [(s1, here_row, 0, side), (rx.at[1], 0, 0, side), (ry.at[2], 0, 0, side)], rows,
    )

    def o_copy(i, landing):
        base = (1 - core if landing else core) * cols + i * side
        dst = gi_out.at[:, pl.ds(pl.multiple_of(base, side), side)]
        return remote(fin.at[:, pl.ds(i * side, side)], dst, o_s.at[i], o_r.at[i], cpart)

    def o_local(i):
        base = pl.multiple_of(core * cols + i * side, side)
        return pltpu.make_async_copy(
            fin.at[:, pl.ds(i * side, side)], gi_out.at[:, pl.ds(base, side)], loc.at[1 + i]
        )

    o_copy(0, False).start()
    o_local(0).start()
    f_copy(0, True).wait_recv()
    f_copy(2, False).start()
    y_copy(1).wait_recv()
    x_copy(2).wait_recv()
    total(
        (fin, 0, side, side),
        [(s1, here_row, side, side), (ry.at[1], 0, 0, side), (rx.at[2], 0, 0, side)], rows,
    )
    o_copy(1, False).start()
    o_local(1).start()

    for i in range(4):
        core_copy(i).wait_send()
    for i in range(3):
        x_copy(i).wait_send()
        y_copy(i).wait_send()
        f_copy(i, False).wait_send()
    f_copy(1, True).wait_recv()
    f_copy(2, True).wait_recv()
    for i in range(2):
        o_copy(i, True).wait_recv()
        o_copy(i, False).wait_send()
        o_local(i).wait()
    own_g.wait()
    for zt in range(line):
        if zt > 0:
            pl.when(z < zt)(lambda: up_copy(zt, True).wait_send())
        if zt < line - 1:
            pl.when(z > zt)(lambda: dn_copy(zt, True).wait_send())


def reduced(part, grad_part):
    line = lax.axis_size("fs") // 2
    rows, cols = part.shape[0] // 4, part.shape[1] // 2
    depth, width = grad_part.shape
    kind = part.dtype
    dma = pltpu.SemaphoreType.DMA
    vmem = pl.BlockSpec(memory_space=pltpu.VMEM)
    anyspec = pl.BlockSpec(memory_space=pl.ANY)
    unit = pltpu.VMEM((3, rows, cols // 2), kind)
    whole = pltpu.VMEM((depth, width), kind)
    return pl.pallas_call(
        functools.partial(reduce_kernel, line),
        out_shape=(
            jax.ShapeDtypeStruct((rows, 2 * cols), kind),
            jax.ShapeDtypeStruct((depth // (2 * line), 4 * width), kind),
        ),
        in_specs=[anyspec, vmem],
        out_specs=(anyspec, anyspec),
        scratch_shapes=[
            pltpu.VMEM((4 * rows, cols), kind),
            pltpu.VMEM((4 * rows, cols), kind),
            pltpu.VMEM((4 * rows, cols), kind),
            unit, unit,
            pltpu.VMEM((2, rows, cols // 2), kind),
            pltpu.VMEM((rows, cols), kind),
            whole, whole, whole, whole,
            pltpu.VMEM((depth // line, width), kind),
            dma((4,)), dma((4,)), dma((3,)), dma((3,)), dma((3,)), dma((3,)),
            dma((line,)), dma((line,)), dma((line,)), dma((line,)),
            dma((3,)), dma((3,)), dma((2,)), dma((2,)), dma((7,)),
        ],
        compiler_params=pltpu.CompilerParams(
            collective_id=1, has_side_effects=True, vmem_limit_bytes=56 * 2**20
        ),
        name="reduce_all",
    )(part, grad_part)


def on_device(inputs, cotangent, gate_weight, up_weight, down_weight):
    tok_rows = inputs.shape[0]
    fs_size = lax.axis_size("fs")
    rep_size = lax.axis_size("rep")
    contract = (((1,), (1,)), ((), ()))
    contract_tok = (((0,), (0,)), ((), ()))
    width = gate_weight.shape[1] // 4
    gate_up, down_full, tokens = gather(
        gate_weight, up_weight, down_weight, inputs, cotangent
    )
    gate_up_val = jnp.dot(tokens[0], gate_up, preferred_element_type=jnp.float32)
    gate_val, up_val = gate_up_val[:, :width], gate_up_val[:, width:]
    grad_hidden = jnp.dot(tokens[1], down_full, preferred_element_type=jnp.float32)
    sigmoid_gate = jax.nn.sigmoid(gate_val)
    active = gate_val * sigmoid_gate
    hidden = (active * up_val).astype(jnp.bfloat16)
    grad_gate = (
        grad_hidden * up_val * sigmoid_gate * (1.0 + gate_val * (1.0 - sigmoid_gate))
    ).astype(jnp.bfloat16)
    grad_up = (grad_hidden * active).astype(jnp.bfloat16)
    grad_scale = 1.0 / math.sqrt(tok_rows * fs_size * rep_size)
    pairs = [[i, i + 1] for i in range(0, fs_size, 2)]
    lines = [list(range(i, fs_size, 2)) for i in range(2)]
    grad_part = lax.dot_general(
        tokens[1], hidden, contract_tok, preferred_element_type=jnp.float32
    )
    part = lax.dot_general(
        jnp.concatenate([grad_gate, grad_up], axis=1), gate_up, contract,
        preferred_element_type=jnp.float32,
    )
    if lax.axis_size("tp") == 2:
        grad_input, grad_down = reduced(
            part.astype(jnp.bfloat16), grad_part.astype(jnp.bfloat16)
        )
        return (grad_input, grad_down.astype(jnp.float32) * grad_scale)
    shard = lax.psum_scatter(
        grad_part.astype(jnp.bfloat16), "fs", scatter_dimension=0, tiled=True,
        axis_index_groups=lines,
    ).astype(jnp.float32) * grad_scale
    shard = lax.all_to_all(
        shard, "fs", split_axis=0, concat_axis=1, tiled=True, axis_index_groups=pairs
    )
    grad_down = lax.all_gather(shard, "rep", axis=1, tiled=True)
    part = lax.psum_scatter(
        part.astype(jnp.bfloat16), "rep", scatter_dimension=0, tiled=True
    )
    part = lax.psum_scatter(
        part, "fs", scatter_dimension=0, tiled=True, axis_index_groups=pairs
    )
    grad_input = lax.psum(part, "tp")
    return (grad_input, grad_down)


def solution(mesh):
    placed = (
        P(("rep", "fs"), None),
        P(("rep", "fs"), None),
        P("fs", "tp"),
        P("fs", "tp"),
        P("fs", "tp"),
    )
    return jax.shard_map(
        on_device,
        mesh=mesh,
        in_specs=placed,
        out_specs=(P(("rep", "fs"), None), P("fs", "tp")),
        check_vma=False,
    )
```

profile of v0, /device:TPU:0, one launch (start us, length us, event | category | flops | bytes accessed | tf_op | source)
XLA Modules:
  0.0 223.5 jit_solution(10615940661789775671)
XLA Ops:
  0.6 107.7 %gather_all.1 = (bf16[2048,1024]{1,0:T(8,128)(2,1)}, bf16[2048,512]{1,0:T(8,128)(2,1)}, bf16[2,2048,2048]{2,1,0:T(8,128)(2,1)}) custom-call(bf16[256,2048]{1,0:T(8,128)(2,1)} %gate_w.1, bf16[256,2048]{1,0:T(8,128)(2,1)} %up_w.1, bf16[256,2048]{1,0:T(8,128)(2,1)} %down_w.1, bf16[512,2048]{1,0:T(8,128)(2,1)} %toks.1, bf16[512,2048]{1,0:T(8,128)(2,1)} %cots.1), custom_call_target="tpu_custom_call" | custom-call | tf_op jit(solution)/shard_map/gather_all/pallas_call | solution.py:199
  108.3 0.0 copy-start.1
  108.3 14.7 %fusion = f32[2048,1024]{0,1:T(8,128)} fusion(bf16[2048,1024]{1,0:T(8,128)(2,1)} %get-tuple-element.9, bf16[2,2048,2048]{2,1,0:T(8,128)(2,1)} %get-tuple-element.7), kind=kOutput, calls=%fused_computation | convolution fusion | flops 8589934592 | bytes 20971520 | tf_op jit(solution)/shard_map/dot_general | solution.py:494
  123.0 0.0 copy-done.1
  123.0 0.0 copy-start.2
  123.0 10.0 %fusion.13.g_in = bf16[2048,512]{1,0:T(8,128)(2,1)} fusion(bf16[2,2048,2048]{2,1,0:T(8,128)(2,1)S(1)} %copy-done.1, f32[2048,1024]{0,1:T(8,128)} %fusion), kind=kOutput, calls=%fused_computation.18 | convolution fusion | flops 4302307328 | bytes 18874368 | tf_op jit(solution)/shard_map/dot_general | solution.py:507
  133.0 0.0 copy-done.2
  133.0 9.8 %multiply_convert_fusion.2 = (bf16[2048,512]{0,1:T(8,128)(2,1)}, bf16[2048,512]{0,1:T(8,128)(2,1)}) fusion(f32[2048,1024]{0,1:T(8,128)} %fusion, bf16[2048,512]{1,0:T(8,128)(2,1)S(1)} %copy-done.2, bf16[2,2048,2048]{2,1,0:T(8,128)(2,1)S(1)} %copy-done.1), kind=kOutput, calls=%fused_computation.15 | convolution fusion | flops 4308598784 | bytes 23068672 | tf_op jit(solution)/shard_map/dot_general | solution.py:496
  142.8 13.9 %convolution_convert_fusion.p_in = bf16[2048,2048]{1,0:T(8,128)(2,1)} fusion(bf16[2048,1024]{1,0:T(8,128)(2,1)} %get-tuple-element.9, bf16[2048,512]{0,1:T(8,128)(2,1)} %get-tuple-element.13, bf16[2048,512]{0,1:T(8,128)(2,1)} %get-tuple-element.12), kind=kOutput, calls=%fused_computation.7 | convolution fusion | flops 8602517504 | bytes 16777216 | tf_op jit(solution)/shard_map/dot_general | solution.py:510
  156.8 62.4 %reduce_all.1 = (bf16[512,2048]{1,0:T(8,128)(2,1)}, bf16[256,2048]{1,0:T(8,128)(2,1)}) custom-call(bf16[2048,2048]{1,0:T(8,128)(2,1)} %convolution_convert_fusion.p_in, bf16[2048,512]{1,0:T(8,128)(2,1)} %fusion.13.g_in), custom_call_target="tpu_custom_call" | custom-call | tf_op jit(solution)/shard_map/reduce_all/pallas_call | solution.py:456
  219.2 0.0 copy-start
  219.2 2.9 %convert_multiply_fusion = f32[256,2048]{1,0:T(8,128)} fusion(bf16[256,2048]{1,0:T(8,128)(2,1)} %get-tuple-element.11), kind=kLoop, calls=%fused_computation.19 | loop fusion | flops 1048576 | bytes 3145728 | tf_op jit(solution)/shard_map/mul | solution.py:518
  222.2 0.0 copy-done
  222.2 1.3 copy.8
Async XLA Ops:
  108.3 14.7 %copy-start.1 = (bf16[2,2048,2048]{2,1,0:T(8,128)(2,1)S(1)}, bf16[2,2048,2048]{2,1,0:T(8,128)(2,1)}, u32[]{:S(2)}) copy-start(bf16[2,2048,2048]{2,1,0:T(8,128)(2,1)} %get-tuple-element.7) | copy-start | bytes 50331652
  123.0 10.0 %copy-start.2 = (bf16[2048,512]{1,0:T(8,128)(2,1)S(1)}, bf16[2048,512]{1,0:T(8,128)(2,1)}, u32[]{:S(2)}) copy-start(bf16[2048,512]{1,0:T(8,128)(2,1)} %get-tuple-element.8) | copy-start | bytes 6291460
  219.2 3.0 %copy-start = (bf16[512,2048]{1,0:T(8,128)(2,1)S(1)}, bf16[512,2048]{1,0:T(8,128)(2,1)}, u32[]{:S(2)}) copy-start(bf16[512,2048]{1,0:T(8,128)(2,1)} %get-tuple-element.16) | copy-start | bytes 6291460
where the time goes:
time: 224 us; the launch traced here: 223 us
  Pallas kernels  170 us (76%)
  matrix products  48.5 us (22%)
  other arithmetic  2.95 us (1%)
    pallas_call x1, Pallas kernels, gather(): pl.pallas_call(functools.partial(gather_kernel, line, units), out_shape=(...  108 us
    pallas_call x1, Pallas kernels, reduced(): pl.pallas_call(functools.partial(reduce_kernel, line), out_shape=(jax.Sha...  62.4 us
    dot_general x1, matrix products, on_device(): jnp.dot(tokens[0], gate_up, preferred_element_type=jnp.float32)  14.7 us
    dot_general x1, matrix products, on_device(): lax.dot_general(jnp.concatenate([grad_gate, grad_up], axis=1), gate_up, c...  13.9 us
    dot_general x1, matrix products, on_device(): lax.dot_general(tokens[1], hidden, contract_tok, preferred_element_type=j...  9.96 us
    dot_general x1, matrix products, on_device(): jnp.dot(tokens[1], down_full, preferred_element_type=jnp.float32)  9.82 us

commit v1 on v0

v1 whole, which is shorter than its diff:
```python
import functools
import math

import jax
import jax.numpy as jnp
from jax import lax
from jax.experimental import pallas as pl
from jax.experimental.pallas import tpu as pltpu
from jax.sharding import PartitionSpec as P

MESH = pl.DeviceIdType.MESH


def fused_kernel(
    line, gate_w, up_w, down_w, toks, cots, gi_out, gd_out,
    x, gu, dn_w, acc, hid, ggu, r1, rx, ry, s3, fin, g, u_in, d_in, gfin,
    up_s, up_r, dn_s, dn_r, wy_s, wy_r, tok_s, tok_r, d2d_s, d2d_r, loc,
    c_s, c_r, x_s, x_r, yy_s, yy_r, u_s, u_r, d_s, d_r, f_s, f_r, o_s, o_r, out_l,
):
    r = lax.axis_index("rep")
    f = lax.axis_index("fs")
    core = lax.axis_index("tp")
    z, y = f // 2, f % 2
    rows = toks.shape[0]
    half = rows // 2
    wrows = gate_w.shape[0]
    width = gate_w.shape[1] // 4
    depth = 2 * line * wrows
    zrows = 2 * wrows
    cols = depth // 2
    side = cols // 2
    frows = wrows
    last = line - 2
    has_up, has_dn = z < line - 1, z > 0
    is_end = (z == 0) | (z == line - 1)
    up = {"fs": (f + 2) % (2 * line)}
    dn = {"fs": (f + 2 * line - 2) % (2 * line)}
    ypart = {"fs": f + 1 - 2 * y}
    xpart = {"rep": 1 - r}
    cpart = {"tp": 1 - core}

    barrier = pltpu.get_barrier_semaphore()
    for dev in (ypart, xpart, cpart, up, dn):
        pl.semaphore_signal(barrier, inc=1, device_id=dev, device_id_type=MESH)
    pl.semaphore_wait(barrier, 5)

    def remote(src, dst, s, q, dev):
        return pltpu.make_async_remote_copy(
            src_ref=src, dst_ref=dst, send_sem=s, recv_sem=q,
            device_id=dev, device_id_type=MESH,
        )

    def wblk(k, zz, yy):
        row = pl.multiple_of((2 * zz + yy) * wrows, wrows)
        if k == 2:
            return dn_w.at[pl.ds(row, wrows), :]
        return gu.at[pl.ds(row, wrows), pl.ds(k * width, width)]

    def own(k, yy):
        col = pl.multiple_of((2 * r + yy) * width, width)
        return (gate_w, up_w, down_w)[k].at[:, pl.ds(col, width)]

    def to_y(k):
        return remote(own(k, 1 - y), wblk(k, z, y), wy_s.at[k], wy_r.at[k], ypart)

    def from_y(k):
        return remote(own(k, 1 - y), wblk(k, z, 1 - y), wy_s.at[k], wy_r.at[k], ypart)

    def zcopy(up_dir, d, sub, k, zz):
        yy = y if sub == 0 else 1 - y
        src = own(k, y) if (d == 0 and sub == 0) else wblk(k, zz, yy)
        s, q, dev = (up_s, up_r, up) if up_dir else (dn_s, dn_r, dn)
        return remote(src, wblk(k, zz, yy), s.at[d, sub, k], q.at[d, sub, k], dev)

    def pred_send(up_dir, d):
        return (has_up & (z - d >= 0)) if up_dir else (has_dn & (z + d <= line - 1))

    def src_z(up_dir, d):
        return jnp.maximum(z - d, 0) if up_dir else jnp.minimum(z + d, line - 1)

    def send(up_dir, d, sub, k):
        @pl.when(pred_send(up_dir, d))
        def _():
            zcopy(up_dir, d, sub, k, src_z(up_dir, d)).start()

    def await_send(up_dir, d, sub, k):
        @pl.when(pred_send(up_dir, d))
        def _():
            zcopy(up_dir, d, sub, k, src_z(up_dir, d)).wait_send()

    def await_recv(up_dir, d, sub, k):
        ok = (z - d - 1 >= 0) if up_dir else (z + d + 1 <= line - 1)

        @pl.when(ok)
        def _():
            zcopy(up_dir, d, sub, k, src_z(up_dir, d + 1)).wait_recv()

    def hop(d, sub, k):
        for up_dir in (True, False):
            await_recv(up_dir, d, sub, k)
            if d < last:
                send(up_dir, d + 1, sub, k)

    def slot(rr, yy):
        return pl.multiple_of((2 * rr + yy) * rows, rows)

    def tblk(j, rr, yy, c):
        row = pl.multiple_of((2 * rr + yy) * rows + c * half, half)
        return x.at[j, pl.ds(row, half), :]

    def mine(j):
        src = toks if j == 0 else cots
        return src.at[pl.ds(pl.multiple_of(core * half, half), half), :]

    def tcopy(i, landing):
        j = (0, 1, 0, 1, 0, 1)[i]
        dev = xpart if i in (0, 1, 4) else ypart
        if landing:
            rr = (1 - r, 1 - r, r, r, 1 - r, 1 - r)[i]
            yy = (y, y, 1 - y, 1 - y, 1 - y, 1 - y)[i]
            src = dst = tblk(j, rr, yy, core)
        else:
            rr = (r, r, r, r, r, 1 - r)[i]
            yy = (y, y, y, y, 1 - y, y)[i]
            dst = tblk(j, rr, yy, core)
            src = mine(j) if i < 4 else dst
        return remote(src, dst, tok_s.at[i], tok_r.at[i], dev)

    def dcopy(i, c):
        j = (0, 1, 0, 1, 0, 1)[i]
        rr = (1 - r, 1 - r, r, r, 1 - r, 1 - r)[i]
        yy = (y, y, 1 - y, 1 - y, 1 - y, 1 - y)[i]
        blk = tblk(j, rr, yy, c)
        return remote(blk, blk, d2d_s.at[i], d2d_r.at[i], cpart)

    def event(i):
        tcopy(i, True).wait_recv()
        if i == 2:
            tcopy(4, False).start()
        if i == 1:
            tcopy(5, False).start()
        dcopy(i, core).start()

    trow = slot(r, y)
    loads = [
        pltpu.make_async_copy(own(0, y), wblk(0, z, y), loc.at[0]),
        pltpu.make_async_copy(own(1, y), wblk(1, z, y), loc.at[1]),
        pltpu.make_async_copy(own(2, y), wblk(2, z, y), loc.at[2]),
        pltpu.make_async_copy(toks, x.at[0, pl.ds(trow, rows), :], loc.at[3]),
        pltpu.make_async_copy(cots, x.at[1, pl.ds(trow, rows), :], loc.at[4]),
    ]

    tile = 256
    z_lo = jnp.maximum(z - last, 0)
    z_hi = jnp.minimum(z + last, line - 1) + 1

    def product(j, row, k0, kk, w, wcol, acol, n):
        at = pl.ds(pl.multiple_of(row, rows), rows)
        kat = pl.ds(pl.multiple_of(k0, wrows), kk)
        for c in range(0, n, tile):
            one = jnp.dot(
                x[j, at, kat], w[kat, pl.ds(wcol + c, tile)],
                preferred_element_type=jnp.float32,
            )
            acc[at, pl.ds(acol + c, tile)] += one

    def forward(j, w, acol, n, first, count):
        @pl.loop(first, first + count)
        def _(b):
            row = ((2 * r + y) + 2 * (b % 2) * (1 - 2 * r) + (b // 2) * (1 - 2 * y)) * rows

            @pl.loop(z_lo, z_hi)
            def _(zz):
                product(j, row, zz * zrows, zrows, w, 0, acol, n)

    def forward_end(j, k, sub):
        for up_dir in (True, False):
            await_recv(up_dir, last, sub, k)

        @pl.when(is_end)
        def _():
            zz = line - 1 - z
            yy = y if sub == 0 else 1 - y
            w = dn_w if k == 2 else gu

            @pl.loop(0, 4)
            def _(b):
                product(
                    j, b * rows, (2 * zz + yy) * wrows, wrows, w,
                    0 if k == 2 else k * width, k * width, width,
                )

    def total(dst, terms, count, step=64):
        @pl.loop(0, count // step)
        def _(i):
            at = pl.multiple_of(i * step, step)
            value = None
            for ref, row, col, wide in terms:
                one = ref[pl.ds(row + at, step), pl.ds(col, wide)].astype(jnp.float32)
                value = one if value is None else value + one
            ref, row, col, wide = dst
            ref[pl.ds(row + at, step), pl.ds(col, wide)] = value.astype(ref.dtype)

    for k in (0, 1):
        to_y(k).start()
        send(True, 0, 0, k)
        send(False, 0, 0, k)
    tcopy(0, False).start()
    tcopy(2, False).start()
    to_y(2).start()
    tcopy(1, False).start()
    tcopy(3, False).start()
    for copy in loads:
        copy.start()

    @pl.loop(0, 4 * rows // 64)
    def _(i):
        at = pl.ds(pl.multiple_of(i * 64, 64), 64)
        acc[at, :] = jnp.zeros((64, 3 * width), jnp.float32)

    for k in (0, 1):
        from_y(k).wait_recv()
        send(True, 0, 1, k)
        send(False, 0, 1, k)
    for sub in range(2):
        for k in (0, 1):
            if last > 0:
                hop(0, sub, k)
    event(0)
    event(2)
    for d in range(1, last):
        for sub in range(2):
            for k in (0, 1):
                hop(d, sub, k)
    send(True, 0, 0, 2)
    send(False, 0, 0, 2)
    from_y(2).wait_recv()
    send(True, 0, 1, 2)
    send(False, 0, 1, 2)
    event(1)
    for load in loads:
        load.wait()
    dcopy(0, 1 - core).wait_recv()
    dcopy(2, 1 - core).wait_recv()
    forward(0, gu, 0, 2 * width, 0, 3)
    for d in range(last):
        for sub in range(2):
            hop(d, sub, 2)
    event(3)
    event(4)
    dcopy(4, 1 - core).wait_recv()
    forward(0, gu, 0, 2 * width, 3, 1)
    for sub in range(2):
        for k in (0, 1):
            forward_end(0, k, sub)

    @pl.loop(0, 4 * rows // 32)
    def _(i):
        at = pl.ds(pl.multiple_of(i * 32, 32), 32)
        gate = acc[at, pl.ds(0, width)]
        up_val = acc[at, pl.ds(width, width)]
        sig = jax.nn.sigmoid(gate)
        active = gate * sig
        hid[at, :] = (active * up_val).astype(hid.dtype)
        acc[at, pl.ds(0, width)] = up_val * sig * (1.0 + gate * (1.0 - sig))
        acc[at, pl.ds(width, width)] = active

    event(5)
    for i in (1, 3, 5):
        dcopy(i, 1 - core).wait_recv()

    def block(ref, zt):
        return ref.at[pl.ds(zt * zrows, zrows), :]

    def up_copy(zt, first):
        return remote(block(g if first else u_in, zt), block(u_in, zt), u_s.at[zt], u_r.at[zt], up)

    def dn_copy(zt, first):
        return remote(block(g if first else d_in, zt), block(d_in, zt), d_s.at[zt], d_r.at[zt], dn)

    for i in range(line):
        zt = jnp.where(z < line // 2, line - 1 - i, i)

        @pl.loop(0, zrows // tile)
        def _(m):
            at = pl.multiple_of(zt * zrows + m * tile, tile)
            one = lax.dot_general(
                x[1, :, pl.ds(at, tile)], hid[...], (((0,), (0,)), ((), ())),
                preferred_element_type=jnp.float32,
            )
            g[pl.ds(at, tile), :] = one.astype(g.dtype)

        if i < line - 1:
            @pl.when(z == 0)
            def _():
                up_copy(line - 1 - i, True).start()

            @pl.when(z == line - 1)
            def _():
                dn_copy(i, True).start()

    def line_step(i):
        zt = line - 1 - i
        if zt > 0:
            @pl.when((z > 0) & (z < zt))
            def _():
                up_copy(zt, False).wait_recv()
                row = zt * zrows
                total((u_in, row, 0, width), [(g, row, 0, width), (u_in, row, 0, width)], zrows)
                up_copy(zt, False).start()

            zd = i

            @pl.when((z < line - 1) & (z > zd))
            def _():
                dn_copy(zd, False).wait_recv()
                row = zd * zrows
                total((d_in, row, 0, width), [(g, row, 0, width), (d_in, row, 0, width)], zrows)
                dn_copy(zd, False).start()

    forward(1, dn_w, 2 * width, width, 0, 4)
    for sub in range(2):
        forward_end(1, 2, sub)

    for i in (0, 2, 4):
        dcopy(i, core).wait_send()
    tcopy(4, False).wait_send()
    order = [(1 - r, 1 - y), (1 - r, y), (r, 1 - y), (r, y)]
    my_col = pl.multiple_of(core * cols, cols)
    its_col = pl.multiple_of((1 - core) * cols, cols)
    part = x.at[0]

    def slopes(row):
        @pl.loop(0, rows // 32)
        def _(i):
            at = pl.ds(pl.multiple_of(row + i * 32, 32), 32)
            grad = acc[at, pl.ds(2 * width, width)]
            ggu[at, pl.ds(0, width)] = (grad * acc[at, pl.ds(0, width)]).astype(ggu.dtype)
            ggu[at, pl.ds(width, width)] = (grad * acc[at, pl.ds(width, width)]).astype(ggu.dtype)

    def back(row, col):
        @pl.loop(0, cols // tile)
        def _(n):
            at = pl.multiple_of(col + n * tile, tile)
            one = lax.dot_general(
                ggu[pl.ds(row, rows), :], gu[pl.ds(at, tile), :], (((1,), (1,)), ((), ())),
                preferred_element_type=jnp.float32,
            )
            x[0, pl.ds(row, rows), pl.ds(at, tile)] = one.astype(x.dtype)

    def core_copy(i):
        at = pl.ds(slot(*order[i]), rows)
        return remote(part.at[at, pl.ds(its_col, cols)], r1.at[at, :], c_s.at[i], c_r.at[i], cpart)

    def s1_half(i, second):
        col = pl.multiple_of(my_col + (side if second else 0), side)
        return part.at[pl.ds(slot(*order[i]), rows), pl.ds(col, side)]

    def s1(row, second):
        return (part, row, pl.multiple_of(my_col + (side if second else 0), side), side)

    def x_copy(i):
        src = s3.at[1] if i == 2 else s1_half(i, False)
        return remote(src, rx.at[i], x_s.at[i], x_r.at[i], xpart)

    def y_copy(i):
        src = s3.at[0] if i == 2 else s1_half((0, 2)[i], True)
        return remote(src, ry.at[i], yy_s.at[i], yy_r.at[i], ypart)

    for i in range(4):
        row = slot(*order[i])
        slopes(row)
        back(row, its_col)
        core_copy(i).start()
        back(row, my_col)
        core_copy(i).wait_recv()
        total((part, row, my_col, cols), [(part, row, my_col, cols), (r1, row, 0, cols)], rows)
        if i in (0, 1):
            x_copy(i).start()
        if i == 0:
            y_copy(0).start()
        if i == 2:
            y_copy(1).start()
        if i < line - 1:
            line_step(i)

    x_copy(0).wait_recv()
    total((s3.at[0], 0, 0, side), [s1(slot(r, 1 - y), False), (rx.at[0], 0, 0, side)], rows)
    y_copy(2).start()
    y_copy(0).wait_recv()
    total((s3.at[1], 0, 0, side), [s1(slot(1 - r, y), True), (ry.at[0], 0, 0, side)], rows)
    x_copy(2).start()
    for i in range(4, line - 1):
        line_step(i)

    zrow = pl.multiple_of(z * zrows, zrows)

    def here(ref):
        return (ref, zrow, 0, width)

    @pl.when(z == 0)
    def _():
        dn_copy(0, True).wait_recv()
        total((gfin, 0, 0, width), [here(g), here(d_in)], zrows)

    @pl.when(z == line - 1)
    def _():
        up_copy(line - 1, True).wait_recv()
        total((gfin, 0, 0, width), [here(g), here(u_in)], zrows)

    @pl.when((z > 0) & (z < line - 1))
    def _():
        remote(block(g, z), block(u_in, z), u_s.at[z], u_r.at[z], up).wait_recv()
        remote(block(g, z), block(d_in, z), d_s.at[z], d_r.at[z], dn).wait_recv()
        total((gfin, 0, 0, width), [here(g), here(u_in), here(d_in)], zrows)

    def gcols(rr, yy):
        return gd_out.at[:, pl.ds(pl.multiple_of((2 * rr + yy) * width, width), width)]

    def grows(yy):
        return gfin.at[pl.ds(pl.multiple_of(yy * frows, frows), frows), :]

    def f_copy(i, landing):
        if i == 0:
            dst = gcols(r, 1 - y) if landing else gcols(r, y)
            return remote(grows(1 - y), dst, f_s.at[0], f_r.at[0], ypart)
        if i == 1:
            dst = gcols(1 - r, y) if landing else gcols(r, y)
            return remote(grows(y), dst, f_s.at[1], f_r.at[1], xpart)
        dst = gcols(1 - r, 1 - y) if landing else gcols(r, 1 - y)
        return remote(gcols(r, 1 - y), dst, f_s.at[2], f_r.at[2], xpart)

    f_copy(0, False).start()
    f_copy(1, False).start()
    own_g = pltpu.make_async_copy(grows(y), gcols(r, y), out_l.at[0])
    own_g.start()

    x_copy(1).wait_recv()
    y_copy(2).wait_recv()
    here_row = slot(r, y)
    total(
        (fin, 0, 0, side),
        [s1(here_row, False), (rx.at[1], 0, 0, side), (ry.at[2], 0, 0, side)], rows,
    )

    def o_copy(i, landing):
        base = (1 - core if landing else core) * cols + i * side
        dst = gi_out.at[:, pl.ds(pl.multiple_of(base, side), side)]
        return remote(fin.at[:, pl.ds(i * side, side)], dst, o_s.at[i], o_r.at[i], cpart)

    def o_local(i):
        base = pl.multiple_of(core * cols + i * side, side)
        return pltpu.make_async_copy(
            fin.at[:, pl.ds(i * side, side)], gi_out.at[:, pl.ds(base, side)], out_l.at[1 + i]
        )

    o_copy(0, False).start()
    o_local(0).start()
    f_copy(0, True).wait_recv()
    f_copy(2, False).start()
    y_copy(1).wait_recv()
    x_copy(2).wait_recv()
    total(
        (fin, 0, side, side),
        [s1(here_row, True), (ry.at[1], 0, 0, side), (rx.at[2], 0, 0, side)], rows,
    )
    o_copy(1, False).start()
    o_local(1).start()

    for i in range(6):
        if i in (1, 3, 5):
            dcopy(i, core).wait_send()
        if i != 4:
            tcopy(i, False).wait_send()
    for k in range(3):
        to_y(k).wait_send()
        for d in range(line - 1):
            for sub in range(2):
                await_send(True, d, sub, k)
                await_send(False, d, sub, k)
    for i in range(4):
        core_copy(i).wait_send()
    for i in range(3):
        x_copy(i).wait_send()
        y_copy(i).wait_send()
        f_copy(i, False).wait_send()
    f_copy(1, True).wait_recv()
    f_copy(2, True).wait_recv()
    for i in range(2):
        o_copy(i, True).wait_recv()
        o_copy(i, False).wait_send()
        o_local(i).wait()
    own_g.wait()
    for zt in range(line):
        if zt > 0:
            pl.when(z < zt)(lambda: up_copy(zt, True).wait_send())
        if zt < line - 1:
            pl.when(z > zt)(lambda: dn_copy(zt, True).wait_send())


def fused(gate_w, up_w, down_w, toks, cots):
    line = lax.axis_size("fs") // 2
    rows, full = toks.shape
    wrows, width = gate_w.shape[0], gate_w.shape[1] // 4
    depth = 2 * line * wrows
    cols = full // 2
    kind = gate_w.dtype
    dma = pltpu.SemaphoreType.DMA
    zsem = dma((line - 1, 2, 3))
    anyspec = pl.BlockSpec(memory_space=pl.ANY)
    whole = pltpu.VMEM((depth, width), kind)
    unit = pltpu.VMEM((3, rows, cols // 2), kind)
    return pl.pallas_call(
        functools.partial(fused_kernel, line),
        out_shape=(
            jax.ShapeDtypeStruct((rows, full), kind),
            jax.ShapeDtypeStruct((wrows, 4 * width), kind),
        ),
        in_specs=[anyspec] * 5,
        out_specs=(anyspec,) * 2,
        scratch_shapes=[
            pltpu.VMEM((2, 4 * rows, full), kind),
            pltpu.VMEM((depth, 2 * width), kind),
            whole,
            pltpu.VMEM((4 * rows, 3 * width), jnp.float32),
            pltpu.VMEM((4 * rows, width), kind),
            pltpu.VMEM((4 * rows, 2 * width), kind),
            pltpu.VMEM((4 * rows, cols), kind),
            unit, unit,
            pltpu.VMEM((2, rows, cols // 2), kind),
            pltpu.VMEM((rows, cols), kind),
            whole, whole, whole,
            pltpu.VMEM((2 * wrows, width), kind),
            zsem, zsem, zsem, zsem,
            dma((3,)), dma((3,)),
            dma((6,)), dma((6,)), dma((6,)), dma((6,)), dma((5,)),
            dma((4,)), dma((4,)), dma((3,)), dma((3,)), dma((3,)), dma((3,)),
            dma((line,)), dma((line,)), dma((line,)), dma((line,)),
            dma((3,)), dma((3,)), dma((2,)), dma((2,)), dma((3,)),
        ],
        compiler_params=pltpu.CompilerParams(
            collective_id=1, has_side_effects=True, vmem_limit_bytes=67043328
        ),
        name="fused_all",
    )(gate_w, up_w, down_w, toks, cots)


def gather_kernel(
    line, units, gate_w, up_w, down_w, toks, cots, gu_out, d_out, t_out, w_tmp, t_tmp,
    up_s, up_r, dn_s, dn_r, y_s, y_r, tok_s, tok_r, d2d_s, d2d_r, loc, loc2,
):
    r = lax.axis_index("rep")
    f = lax.axis_index("fs")
    t = lax.axis_index("tp")
    z, y = f // 2, f % 2
    rows = toks.shape[0]
    half = rows // 2
    wrows = gate_w.shape[0]
    width = gate_w.shape[1] // 4
    parts = len(units)
    has_up, has_dn = z < line - 1, z > 0
    up = {"fs": (f + 2) % (2 * line)}
    dn = {"fs": (f + 2 * line - 2) % (2 * line)}
    ypart = {"fs": f + 1 - 2 * y}
    xpart = {"rep": 1 - r}
    core = t % 2
    cpart = {"tp": t + 1 - 2 * core}

    barrier = pltpu.get_barrier_semaphore()

    def greet(dev):
        pl.semaphore_signal(barrier, inc=1, device_id=dev, device_id_type=MESH)

    for dev in (ypart, xpart, cpart, up, dn):
        greet(dev)
    pl.semaphore_wait(barrier, 5)

    def remote(src, dst, s, q, dev):
        return pltpu.make_async_remote_copy(
            src_ref=src, dst_ref=dst, send_sem=s, recv_sem=q,
            device_id=dev, device_id_type=MESH,
        )

    def wblk(k, zz, yy):
        row = pl.multiple_of((2 * zz + yy) * wrows, wrows)
        which, col, wide = units[k]
        return (gu_out, d_out)[which].at[pl.ds(row, wrows), pl.ds(col, wide)]

    def own(k, yy):
        col = pl.multiple_of((2 * r + yy) * width, width)
        return (gate_w, up_w, down_w)[k].at[:, pl.ds(col, width)]

    def to_y(k):
        return remote(own(k, 1 - y), wblk(k, z, y), y_s.at[k], y_r.at[k], ypart)

    def from_y(k):
        return remote(own(k, 1 - y), wblk(k, z, 1 - y), y_s.at[k], y_r.at[k], ypart)

    def zcopy(up_dir, d, sub, k, zz):
        yy = y if sub == 0 else 1 - y
        src = own(k, y) if (d == 0 and sub == 0) else wblk(k, zz, yy)
        s, q, dev = (up_s, up_r, up) if up_dir else (dn_s, dn_r, dn)
        return remote(src, wblk(k, zz, yy), s.at[d, sub, k], q.at[d, sub, k], dev)

    def pred_send(up_dir, d):
        return (has_up & (z - d >= 0)) if up_dir else (has_dn & (z + d <= line - 1))

    def src_z(up_dir, d):
        return jnp.maximum(z - d, 0) if up_dir else jnp.minimum(z + d, line - 1)

    def send(up_dir, d, sub, k):
        @pl.when(pred_send(up_dir, d))
        def _():
            zcopy(up_dir, d, sub, k, src_z(up_dir, d)).start()

    def await_send(up_dir, d, sub, k):
        @pl.when(pred_send(up_dir, d))
        def _():
            zcopy(up_dir, d, sub, k, src_z(up_dir, d)).wait_send()

    def await_recv(up_dir, d, sub, k):
        ok = (z - d - 1 >= 0) if up_dir else (z + d + 1 <= line - 1)

        @pl.when(ok)
        def _():
            zcopy(up_dir, d, sub, k, src_z(up_dir, d + 1)).wait_recv()

    def tblk(j, rr, yy, c):
        row = pl.multiple_of((2 * rr + yy) * rows + c * half, half)
        return t_out.at[j, pl.ds(row, half), :]

    def mine(j):
        src = toks if j == 0 else cots
        return src.at[pl.ds(pl.multiple_of(core * half, half), half), :]

    def tcopy(i, landing):
        j = (0, 1, 0, 1, 0, 1)[i]
        dev = xpart if i in (0, 1, 5) else ypart
        if landing:
            rr = (1 - r, 1 - r, r, r, 1 - r, 1 - r)[i]
            yy = (y, y, 1 - y, 1 - y, 1 - y, 1 - y)[i]
            src = dst = tblk(j, rr, yy, core)
        else:
            rr = (r, r, r, r, 1 - r, r)[i]
            yy = (y, y, y, y, y, 1 - y)[i]
            dst = tblk(j, rr, yy, core)
            src = mine(j) if i < 4 else dst
        return remote(src, dst, tok_s.at[i], tok_r.at[i], dev)

    def dcopy(i, c):
        j = (0, 1, 0, 1, 0, 1)[i]
        rr = (1 - r, 1 - r, r, r, 1 - r, 1 - r)[i]
        yy = (y, y, 1 - y, 1 - y, 1 - y, 1 - y)[i]
        blk = tblk(j, rr, yy, c)
        return remote(blk, blk, d2d_s.at[i], d2d_r.at[i], cpart)

    loads = [
        pltpu.make_async_copy(own(0, y), w_tmp.at[0], loc.at[0]),
        pltpu.make_async_copy(own(1, y), w_tmp.at[1], loc.at[3]),
        pltpu.make_async_copy(own(2, y), w_tmp.at[2], loc.at[4]),
        pltpu.make_async_copy(toks, t_tmp.at[0], loc.at[1]),
        pltpu.make_async_copy(cots, t_tmp.at[1], loc.at[2]),
    ]
    trow = pl.multiple_of((2 * r + y) * rows, rows)
    stores = [
        pltpu.make_async_copy(w_tmp.at[0], wblk(0, z, y), loc2.at[0]),
        pltpu.make_async_copy(w_tmp.at[1], wblk(1, z, y), loc2.at[3]),
        pltpu.make_async_copy(w_tmp.at[2], wblk(2, z, y), loc2.at[4]),
        pltpu.make_async_copy(t_tmp.at[0], t_out.at[0, pl.ds(trow, rows), :], loc2.at[1]),
        pltpu.make_async_copy(t_tmp.at[1], t_out.at[1, pl.ds(trow, rows), :], loc2.at[2]),
    ]

    for k in range(parts):
        to_y(k).start()
        send(True, 0, 0, k)
        send(False, 0, 0, k)
    for i in (0, 1, 3, 2):
        tcopy(i, False).start()
    for copy in loads:
        copy.start()
    for load, store in zip(loads, stores):
        load.wait()
        store.start()
    for k in range(parts):
        from_y(k).wait_recv()
        send(True, 0, 1, k)
        send(False, 0, 1, k)

    def event(i):
        tcopy(i, True).wait_recv()
        if i == 0:
            tcopy(4, False).start()
        if i == 3:
            tcopy(5, False).start()
        dcopy(i, core).start()

    events = [0, 3, 1, 2, 5, 4]
    for d in range(line - 1):
        for sub in range(2):
            if events:
                event(events.pop(0))
            for k in range(parts):
                for up_dir in (True, False):
                    await_recv(up_dir, d, sub, k)
                    if d + 1 < line - 1:
                        send(up_dir, d + 1, sub, k)
    for i in events:
        event(i)
    for i in range(6):
        dcopy(i, 1 - core).wait_recv()
        dcopy(i, core).wait_send()
        tcopy(i, False).wait_send()
    for k in range(parts):
        to_y(k).wait_send()
        for d in range(line - 1):
            for sub in range(2):
                await_send(True, d, sub, k)
                await_send(False, d, sub, k)
    for store in stores:
        store.wait()


def gather(gate_w, up_w, down_w, toks, cots):
    line = lax.axis_size("fs") // 2
    wrows, width = gate_w.shape[0], gate_w.shape[1] // 4
    units = [(0, 0, width), (0, width, width), (1, 0, width)]
    parts = len(units)
    depth = 2 * line * wrows
    kind = gate_w.dtype
    dma = pltpu.SemaphoreType.DMA
    zsem = dma((line - 1, 2, parts))
    anyspec = pl.BlockSpec(memory_space=pl.ANY)
    return pl.pallas_call(
        functools.partial(gather_kernel, line, units),
        out_shape=(
            jax.ShapeDtypeStruct((depth, 2 * width), kind),
            jax.ShapeDtypeStruct((depth, width), kind),
            jax.ShapeDtypeStruct((2, 4 * toks.shape[0], toks.shape[1]), toks.dtype),
        ),
        in_specs=[anyspec] * 5,
        out_specs=(anyspec,) * 3,
        scratch_shapes=[
            pltpu.VMEM((parts, wrows, width), kind),
            pltpu.VMEM((2,) + toks.shape, toks.dtype),
            zsem, zsem, zsem, zsem,
            dma((parts,)), dma((parts,)),
            dma((6,)), dma((6,)), dma((6,)), dma((6,)),
            dma((5,)), dma((5,)),
        ],
        compiler_params=pltpu.CompilerParams(collective_id=0, has_side_effects=True),
        name="gather_all",
    )(gate_w, up_w, down_w, toks, cots)


def on_device(inputs, cotangent, gate_weight, up_weight, down_weight):
    tok_rows = inputs.shape[0]
    fs_size = lax.axis_size("fs")
    rep_size = lax.axis_size("rep")
    grad_scale = 1.0 / math.sqrt(tok_rows * fs_size * rep_size)
    if lax.axis_size("tp") == 2:
        grad_input, grad_down = fused(
            gate_weight, up_weight, down_weight, inputs, cotangent
        )
        return (grad_input, grad_down.astype(jnp.float32) * grad_scale)
    contract = (((1,), (1,)), ((), ()))
    contract_tok = (((0,), (0,)), ((), ()))
    width = gate_weight.shape[1] // 4
    gate_up, down_full, tokens = gather(
        gate_weight, up_weight, down_weight, inputs, cotangent
    )
    gate_up_val = jnp.dot(tokens[0], gate_up, preferred_element_type=jnp.float32)
    gate_val, up_val = gate_up_val[:, :width], gate_up_val[:, width:]
    grad_hidden = jnp.dot(tokens[1], down_full, preferred_element_type=jnp.float32)
    sigmoid_gate = jax.nn.sigmoid(gate_val)
    active = gate_val * sigmoid_gate
    hidden = (active * up_val).astype(jnp.bfloat16)
    grad_gate = (
        grad_hidden * up_val * sigmoid_gate * (1.0 + gate_val * (1.0 - sigmoid_gate))
    ).astype(jnp.bfloat16)
    grad_up = (grad_hidden * active).astype(jnp.bfloat16)
    pairs = [[i, i + 1] for i in range(0, fs_size, 2)]
    lines = [list(range(i, fs_size, 2)) for i in range(2)]
    grad_part = lax.dot_general(
        tokens[1], hidden, contract_tok, preferred_element_type=jnp.float32
    )
    part = lax.dot_general(
        jnp.concatenate([grad_gate, grad_up], axis=1), gate_up, contract,
        preferred_element_type=jnp.float32,
    )
    shard = lax.psum_scatter(
        grad_part.astype(jnp.bfloat16), "fs", scatter_dimension=0, tiled=True,
        axis_index_groups=lines,
    ).astype(jnp.float32) * grad_scale
    shard = lax.all_to_all(
        shard, "fs", split_axis=0, concat_axis=1, tiled=True, axis_index_groups=pairs
    )
    grad_down = lax.all_gather(shard, "rep", axis=1, tiled=True)
    part = lax.psum_scatter(
        part.astype(jnp.bfloat16), "rep", scatter_dimension=0, tiled=True
    )
    part = lax.psum_scatter(
        part, "fs", scatter_dimension=0, tiled=True, axis_index_groups=pairs
    )
    grad_input = lax.psum(part, "tp")
    return (grad_input, grad_down)


def solution(mesh):
    placed = (
        P(("rep", "fs"), None),
        P(("rep", "fs"), None),
        P("fs", "tp"),
        P("fs", "tp"),
        P("fs", "tp"),
    )
    return jax.shard_map(
        on_device,
        mesh=mesh,
        in_specs=placed,
        out_specs=(P(("rep", "fs"), None), P("fs", "tp")),
        check_vma=False,
    )
```

time: 224 us -> 197 us (0.88)
  the two profiles are of different devices: /device:TPU:0 before, /device:TPU:8 now
where the time goes in v1:
time: 197 us
  Pallas kernels  192 us (97%)
  other arithmetic  2.95 us (1%)
    pallas_call x1, Pallas kernels, fused(): pl.pallas_call(functools.partial(fused_kernel, line), out_shape=(jax.Shap...  192 us

profile of v1, /device:TPU:8, one launch (start us, length us, event | category | flops | bytes accessed | tf_op | source)
XLA Modules:
  0.0 197.1 jit_solution(8504654984112819836)
XLA Ops:
  0.6 192.2 %fused_all.1 = (bf16[512,2048]{1,0:T(8,128)(2,1)}, bf16[256,2048]{1,0:T(8,128)(2,1)}) custom-call(bf16[256,2048]{1,0:T(8,128)(2,1)} %gate_w.1, bf16[256,2048]{1,0:T(8,128)(2,1)} %up_w.1, bf16[256,2048]{1,0:T(8,128)(2,1)} %down_w.1, bf16[512,2048]{1,0:T(8,128)(2,1)} %toks.1, bf16[512,2048]{1,0:T(8,128)(2,1)} %cots.1), custom_call_target="tpu_custom_call" | custom-call | tf_op jit(solution)/shard_map/fused_all/pallas_call | solution.py:513
  192.9 0.0 copy-start
  192.9 2.9 %convert_multiply_fusion = f32[256,2048]{1,0:T(8,128)} fusion(bf16[256,2048]{1,0:T(8,128)(2,1)} %get-tuple-element.5), kind=kLoop, calls=%fused_computation | loop fusion | flops 1048576 | bytes 3145728 | tf_op jit(solution)/shard_map/mul | solution.py:764
  195.8 0.0 copy-done
  195.8 1.3 copy.8
Async XLA Ops:
  192.9 3.0 %copy-start = (bf16[512,2048]{1,0:T(8,128)(2,1)S(1)}, bf16[512,2048]{1,0:T(8,128)(2,1)}, u32[]{:S(2)}) copy-start(bf16[512,2048]{1,0:T(8,128)(2,1)} %get-tuple-element.8) | copy-start | bytes 6291460

commit v2 on v1

--- a/solution.py
+++ b/solution.py
@@ -12,10 +12,10 @@
 
 
 def fused_kernel(
-    line, gate_w, up_w, down_w, toks, cots, gi_out, gd_out,
-    x, gu, dn_w, acc, hid, ggu, r1, rx, ry, s3, fin, g, u_in, d_in, gfin,
+    line, grad_scale, gate_w, up_w, down_w, toks, cots, gi_out, gd_out,
+    x, gu, dn_w, acc, hid, ggu, r1, rx, ry, s3, fin, g, u_in, d_in, gfin, gl, gs,
     up_s, up_r, dn_s, dn_r, wy_s, wy_r, tok_s, tok_r, d2d_s, d2d_r, loc,
-    c_s, c_r, x_s, x_r, yy_s, yy_r, u_s, u_r, d_s, d_r, f_s, f_r, o_s, o_r, out_l,
+    c_s, c_r, x_s, x_r, yy_s, yy_r, u_s, u_r, d_s, d_r, f_s, f_r, o_s, o_r, out_l, gl_s,
 ):
     r = lax.axis_index("rep")
     f = lax.axis_index("fs")
@@ -95,50 +95,70 @@
         def _():
             zcopy(up_dir, d, sub, k, src_z(up_dir, d + 1)).wait_recv()
 
-    def hop(d, sub, k):
+    def relay(d, sub, k):
         for up_dir in (True, False):
-            await_recv(up_dir, d, sub, k)
-            if d < last:
-                send(up_dir, d + 1, sub, k)
+            @pl.when(pred_send(up_dir, d + 1))
+            def _():
+                zcopy(up_dir, d, sub, k, src_z(up_dir, d + 1)).wait_recv()
+                zcopy(up_dir, d + 1, sub, k, src_z(up_dir, d + 1)).start()
+
+    def settle(d, sub, k):
+        for up_dir in (True, False):
+            ok = (z - d - 1 >= 0) if up_dir else (z + d + 1 <= line - 1)
+            onward = has_up if up_dir else has_dn
+
+            @pl.when(ok & jnp.logical_not(onward))
+            def _():
+                zcopy(up_dir, d, sub, k, src_z(up_dir, d + 1)).wait_recv()
 
     def slot(rr, yy):
         return pl.multiple_of((2 * rr + yy) * rows, rows)
 
-    def tblk(j, rr, yy, c):
-        row = pl.multiple_of((2 * rr + yy) * rows + c * half, half)
-        return x.at[j, pl.ds(row, half), :]
-
-    def mine(j):
-        src = toks if j == 0 else cots
-        return src.at[pl.ds(pl.multiple_of(core * half, half), half), :]
-
-    def tcopy(i, landing):
-        j = (0, 1, 0, 1, 0, 1)[i]
-        dev = xpart if i in (0, 1, 4) else ypart
-        if landing:
-            rr = (1 - r, 1 - r, r, r, 1 - r, 1 - r)[i]
-            yy = (y, y, 1 - y, 1 - y, 1 - y, 1 - y)[i]
-            src = dst = tblk(j, rr, yy, core)
+    kinds = (0, 1, 1, 0, 1, 0, 1, 1)
+    over_x = (True, True, True, False, False, True, False, True)
+    parts = (2, 0, 1, 2, 2, 2, 0, 1)
+    ntok = len(kinds)
+
+    def span(c, p):
+        if p == 2:
+            return c * half, half
+        return c * half + p * (half // 2), half // 2
+
+    def tblk(i, rr, yy, c):
+        at, count = span(c, parts[i])
+        row = pl.multiple_of((2 * rr + yy) * rows + at, half // 2)
+        return x.at[kinds[i], pl.ds(row, count), :]
+
+    def mine(i):
+        at, count = span(core, parts[i])
+        src = toks if kinds[i] == 0 else cots
+        return src.at[pl.ds(pl.multiple_of(at, half // 2), count), :]
+
+    def landing(i, c):
+        rr = (1 - r, 1 - r, 1 - r, r, r, 1 - r, 1 - r, 1 - r)[i]
+        yy = (y, y, y, 1 - y, 1 - y, 1 - y, 1 - y, 1 - y)[i]
+        return tblk(i, rr, yy, c)
+
+    def tcopy(i, land):
+        dev = xpart if over_x[i] else ypart
+        if land:
+            src = dst = landing(i, core)
         else:
-            rr = (r, r, r, r, r, 1 - r)[i]
-            yy = (y, y, y, y, 1 - y, y)[i]
-            dst = tblk(j, rr, yy, core)
-            src = mine(j) if i < 4 else dst
+            rr = (r, r, r, r, r, r, 1 - r, r)[i]
+            yy = (y, y, y, y, y, 1 - y, y, 1 - y)[i]
+            dst = tblk(i, rr, yy, core)
+            src = mine(i) if i < 5 else dst
         return remote(src, dst, tok_s.at[i], tok_r.at[i], dev)
 
     def dcopy(i, c):
-        j = (0, 1, 0, 1, 0, 1)[i]
-        rr = (1 - r, 1 - r, r, r, 1 - r, 1 - r)[i]
-        yy = (y, y, 1 - y, 1 - y, 1 - y, 1 - y)[i]
-        blk = tblk(j, rr, yy, c)
+        blk = landing(i, c)
         return remote(blk, blk, d2d_s.at[i], d2d_r.at[i], cpart)
 
     def event(i):
         tcopy(i, True).wait_recv()
-        if i == 2:
-            tcopy(4, False).start()
-        if i == 1:
-            tcopy(5, False).start()
+        onward = {1: 6, 3: 5, 4: 7}.get(i)
+        if onward is not None:
+            tcopy(onward, False).start()
         dcopy(i, core).start()
 
     trow = slot(r, y)
@@ -205,11 +225,10 @@
         to_y(k).start()
         send(True, 0, 0, k)
         send(False, 0, 0, k)
-    tcopy(0, False).start()
-    tcopy(2, False).start()
+    for i in (0, 1, 3):
+        tcopy(i, False).start()
     to_y(2).start()
-    tcopy(1, False).start()
-    tcopy(3, False).start()
+    tcopy(4, False).start()
     for copy in loads:
         copy.start()
 
@@ -222,34 +241,42 @@
         from_y(k).wait_recv()
         send(True, 0, 1, k)
         send(False, 0, 1, k)
-    for sub in range(2):
-        for k in (0, 1):
-            if last > 0:
-                hop(0, sub, k)
+    if last > 0:
+        for sub in range(2):
+            for k in (0, 1):
+                relay(0, sub, k)
     event(0)
-    event(2)
+    event(3)
+    tcopy(2, False).start()
+    event(1)
     for d in range(1, last):
         for sub in range(2):
             for k in (0, 1):
-                hop(d, sub, k)
+                relay(d, sub, k)
     send(True, 0, 0, 2)
     send(False, 0, 0, 2)
     from_y(2).wait_recv()
     send(True, 0, 1, 2)
     send(False, 0, 1, 2)
-    event(1)
     for load in loads:
         load.wait()
-    dcopy(0, 1 - core).wait_recv()
-    dcopy(2, 1 - core).wait_recv()
-    forward(0, gu, 0, 2 * width, 0, 3)
     for d in range(last):
         for sub in range(2):
-            hop(d, sub, 2)
-    event(3)
+            for k in (0, 1):
+                settle(d, sub, k)
+    dcopy(0, 1 - core).wait_recv()
+    dcopy(3, 1 - core).wait_recv()
+    forward(0, gu, 0, 2 * width, 0, 3)
+    if last > 0:
+        for sub in range(2):
+            relay(0, sub, 2)
+    event(5)
     event(4)
-    dcopy(4, 1 - core).wait_recv()
+    dcopy(5, 1 - core).wait_recv()
     forward(0, gu, 0, 2 * width, 3, 1)
+    for d in range(1, last):
+        for sub in range(2):
+            relay(d, sub, 2)
     for sub in range(2):
         for k in (0, 1):
             forward_end(0, k, sub)
@@ -265,8 +292,9 @@
         acc[at, pl.ds(0, width)] = up_val * sig * (1.0 + gate * (1.0 - sig))
         acc[at, pl.ds(width, width)] = active
 
-    event(5)
-    for i in (1, 3, 5):
+    for i in (2, 6, 7):
+        event(i)
+    for i in (1, 2, 4, 6, 7):
         dcopy(i, 1 - core).wait_recv()
 
     def block(ref, zt):
@@ -281,14 +309,12 @@
     for i in range(line):
         zt = jnp.where(z < line // 2, line - 1 - i, i)
 
-        @pl.loop(0, zrows // tile)
-        def _(m):
-            at = pl.multiple_of(zt * zrows + m * tile, tile)
-            one = lax.dot_general(
-                x[1, :, pl.ds(at, tile)], hid[...], (((0,), (0,)), ((), ())),
-                preferred_element_type=jnp.float32,
-            )
-            g[pl.ds(at, tile), :] = one.astype(g.dtype)
+        at = pl.multiple_of(zt * zrows, zrows)
+        one = lax.dot_general(
+            x[1, :, pl.ds(at, zrows)], hid[...], (((0,), (0,)), ((), ())),
+            preferred_element_type=jnp.float32,
+        )
+        g[pl.ds(at, zrows), :] = one.astype(g.dtype)
 
         if i < line - 1:
             @pl.when(z == 0)
@@ -299,32 +325,36 @@
             def _():
                 dn_copy(i, True).start()
 
-    def line_step(i):
-        zt = line - 1 - i
-        if zt > 0:
-            @pl.when((z > 0) & (z < zt))
-            def _():
-                up_copy(zt, False).wait_recv()
-                row = zt * zrows
-                total((u_in, row, 0, width), [(g, row, 0, width), (u_in, row, 0, width)], zrows)
-                up_copy(zt, False).start()
-
-            zd = i
-
-            @pl.when((z < line - 1) & (z > zd))
-            def _():
-                dn_copy(zd, False).wait_recv()
-                row = zd * zrows
-                total((d_in, row, 0, width), [(g, row, 0, width), (d_in, row, 0, width)], zrows)
-                dn_copy(zd, False).start()
-
+    def line_step(t):
+        zt = line - 1 + z - t
+
+        @pl.when((z > 0) & (zt <= line - 1) & (zt > z))
+        def _():
+            up_copy(zt, False).wait_recv()
+            row = pl.multiple_of(zt * zrows, zrows)
+            total((u_in, row, 0, width), [(g, row, 0, width), (u_in, row, 0, width)], zrows)
+            up_copy(zt, False).start()
+
+        zd = t - (line - 1 - z)
+
+        @pl.when((z < line - 1) & (zd >= 0) & (zd < z))
+        def _():
+            dn_copy(zd, False).wait_recv()
+            row = pl.multiple_of(zd * zrows, zrows)
+            total((d_in, row, 0, width), [(g, row, 0, width), (d_in, row, 0, width)], zrows)
+            dn_copy(zd, False).start()
+
+    for d in range(last):
+        for sub in range(2):
+            settle(d, sub, 2)
     forward(1, dn_w, 2 * width, width, 0, 4)
     for sub in range(2):
         forward_end(1, 2, sub)
 
-    for i in (0, 2, 4):
+    for i in (0, 3, 5):
         dcopy(i, core).wait_send()
-    tcopy(4, False).wait_send()
+    tcopy(5, False).wait_send()
+    line_step(1)
     order = [(1 - r, 1 - y), (1 - r, y), (r, 1 - y), (r, y)]
     my_col = pl.multiple_of(core * cols, cols)
     its_col = pl.multiple_of((1 - core) * cols, cols)
@@ -339,14 +369,14 @@
             ggu[at, pl.ds(width, width)] = (grad * acc[at, pl.ds(width, width)]).astype(ggu.dtype)
 
     def back(row, col):
-        @pl.loop(0, cols // tile)
+        @pl.loop(0, cols // side)
         def _(n):
-            at = pl.multiple_of(col + n * tile, tile)
+            at = pl.multiple_of(col + n * side, side)
             one = lax.dot_general(
-                ggu[pl.ds(row, rows), :], gu[pl.ds(at, tile), :], (((1,), (1,)), ((), ())),
+                ggu[pl.ds(row, rows), :], gu[pl.ds(at, side), :], (((1,), (1,)), ((), ())),
                 preferred_element_type=jnp.float32,
             )
-            x[0, pl.ds(row, rows), pl.ds(at, tile)] = one.astype(x.dtype)
+            x[0, pl.ds(row, rows), pl.ds(at, side)] = one.astype(x.dtype)
 
     def core_copy(i):
         at = pl.ds(slot(*order[i]), rows)
@@ -381,8 +411,70 @@
             y_copy(0).start()
         if i == 2:
             y_copy(1).start()
-        if i < line - 1:
-            line_step(i)
+        if i == 2:
+            for t in range(2, line - 1):
+                line_step(t)
+
+    zrow = pl.multiple_of(z * zrows, zrows)
+
+    def here(ref):
+        return (ref, zrow, 0, width)
+
+    @pl.when(z == 0)
+    def _():
+        dn_copy(0, True).wait_recv()
+        total((gfin, 0, 0, width), [here(g), here(d_in)], zrows)
+
+    @pl.when(z == line - 1)
+    def _():
+        up_copy(line - 1, True).wait_recv()
+        total((gfin, 0, 0, width), [here(g), here(u_in)], zrows)
+
+    @pl.when((z > 0) & (z < line - 1))
+    def _():
+        remote(block(g, z), block(u_in, z), u_s.at[z], u_r.at[z], up).wait_recv()
+        remote(block(g, z), block(d_in, z), d_s.at[z], d_r.at[z], dn).wait_recv()
+        total((gfin, 0, 0, width), [here(g), here(u_in), here(d_in)], zrows)
+
+    def gcol(rr, yy):
+        return pl.multiple_of((2 * rr + yy) * width, width)
+
+    def gcols(rr, yy):
+        return gl.at[:, pl.ds(gcol(rr, yy), width)]
+
+    def grows(yy):
+        return gfin.at[pl.ds(pl.multiple_of(yy * frows, frows), frows), :]
+
+    def f_copy(i, land):
+        if i == 0:
+            src, dst, dev = grows(1 - y), gcols(r, 1 - y) if land else gcols(r, y), ypart
+        elif i == 1:
+            src, dst, dev = grows(y), gcols(1 - r, y) if land else gcols(r, y), xpart
+        else:
+            src, dev = gcols(r, 1 - y), xpart
+            dst = gcols(1 - r, 1 - y) if land else src
+        return remote(src, dst, f_s.at[i], f_r.at[i], dev)
+
+    def scaled(i, ref, row, col, rr, yy):
+        at_col = gcol(rr, yy)
+
+        @pl.loop(0, frows // 64)
+        def _(m):
+            at = pl.multiple_of(m * 64, 64)
+            one = ref[pl.ds(row + at, 64), pl.ds(col, width)].astype(jnp.float32)
+            gs[pl.ds(at, 64), pl.ds(at_col, width)] = one * grad_scale
+
+        g_local(i, rr, yy).start()
+
+    def g_local(i, rr, yy):
+        at = gcol(rr, yy)
+        return pltpu.make_async_copy(
+            gs.at[:, pl.ds(at, width)], gd_out.at[:, pl.ds(at, width)], gl_s.at[i]
+        )
+
+    f_copy(0, False).start()
+    f_copy(1, False).start()
+    scaled(0, gfin, pl.multiple_of(y * frows, frows), 0, r, y)
 
     x_copy(0).wait_recv()
     total((s3.at[0], 0, 0, side), [s1(slot(r, 1 - y), False), (rx.at[0], 0, 0, side)], rows)
@@ -390,50 +482,11 @@
     y_copy(0).wait_recv()
     total((s3.at[1], 0, 0, side), [s1(slot(1 - r, y), True), (ry.at[0], 0, 0, side)], rows)
     x_copy(2).start()
-    for i in range(4, line - 1):
-        line_step(i)
-
-    zrow = pl.multiple_of(z * zrows, zrows)
-
-    def here(ref):
-        return (ref, zrow, 0, width)
-
-    @pl.when(z == 0)
-    def _():
-        dn_copy(0, True).wait_recv()
-        total((gfin, 0, 0, width), [here(g), here(d_in)], zrows)
-
-    @pl.when(z == line - 1)
-    def _():
-        up_copy(line - 1, True).wait_recv()
-        total((gfin, 0, 0, width), [here(g), here(u_in)], zrows)
-
-    @pl.when((z > 0) & (z < line - 1))
-    def _():
-        remote(block(g, z), block(u_in, z), u_s.at[z], u_r.at[z], up).wait_recv()
-        remote(block(g, z), block(d_in, z), d_s.at[z], d_r.at[z], dn).wait_recv()
-        total((gfin, 0, 0, width), [here(g), here(u_in), here(d_in)], zrows)
-
-    def gcols(rr, yy):
-        return gd_out.at[:, pl.ds(pl.multiple_of((2 * rr + yy) * width, width), width)]
-
-    def grows(yy):
-        return gfin.at[pl.ds(pl.multiple_of(yy * frows, frows), frows), :]
-
-    def f_copy(i, landing):
-        if i == 0:
-            dst = gcols(r, 1 - y) if landing else gcols(r, y)
-            return remote(grows(1 - y), dst, f_s.at[0], f_r.at[0], ypart)
-        if i == 1:
-            dst = gcols(1 - r, y) if landing else gcols(r, y)
-            return remote(grows(y), dst, f_s.at[1], f_r.at[1], xpart)
-        dst = gcols(1 - r, 1 - y) if landing else gcols(r, 1 - y)
-        return remote(gcols(r, 1 - y), dst, f_s.at[2], f_r.at[2], xpart)
-
-    f_copy(0, False).start()
-    f_copy(1, False).start()
-    own_g = pltpu.make_async_copy(grows(y), gcols(r, y), out_l.at[0])
-    own_g.start()
+    f_copy(0, True).wait_recv()
+    f_copy(2, False).start()
+    scaled(1, gl, 0, gcol(r, 1 - y), r, 1 - y)
+    f_copy(1, True).wait_recv()
+    scaled(2, gl, 0, gcol(1 - r, y), 1 - r, y)
 
     x_copy(1).wait_recv()
     y_copy(2).wait_recv()
@@ -443,21 +496,19 @@
         [s1(here_row, False), (rx.at[1], 0, 0, side), (ry.at[2], 0, 0, side)], rows,
     )
 
-    def o_copy(i, landing):
-        base = (1 - core if landing else core) * cols + i * side
+    def o_copy(i, land):
+        base = (1 - core if land else core) * cols + i * side
         dst = gi_out.at[:, pl.ds(pl.multiple_of(base, side), side)]
         return remote(fin.at[:, pl.ds(i * side, side)], dst, o_s.at[i], o_r.at[i], cpart)
 
     def o_local(i):
         base = pl.multiple_of(core * cols + i * side, side)
         return pltpu.make_async_copy(
-            fin.at[:, pl.ds(i * side, side)], gi_out.at[:, pl.ds(base, side)], out_l.at[1 + i]
+            fin.at[:, pl.ds(i * side, side)], gi_out.at[:, pl.ds(base, side)], out_l.at[i]
         )
 
     o_copy(0, False).start()
     o_local(0).start()
-    f_copy(0, True).wait_recv()
-    f_copy(2, False).start()
     y_copy(1).wait_recv()
     x_copy(2).wait_recv()
     total(
@@ -466,11 +517,13 @@
     )
     o_copy(1, False).start()
     o_local(1).start()
-
-    for i in range(6):
-        if i in (1, 3, 5):
+    f_copy(2, True).wait_recv()
+    scaled(3, gl, 0, gcol(1 - r, 1 - y), 1 - r, 1 - y)
+
+    for i in range(ntok):
+        if kinds[i] == 1:
             dcopy(i, core).wait_send()
-        if i != 4:
+        if i != 5:
             tcopy(i, False).wait_send()
     for k in range(3):
         to_y(k).wait_send()
@@ -484,13 +537,12 @@
         x_copy(i).wait_send()
         y_copy(i).wait_send()
         f_copy(i, False).wait_send()
-    f_copy(1, True).wait_recv()
-    f_copy(2, True).wait_recv()
     for i in range(2):
         o_copy(i, True).wait_recv()
         o_copy(i, False).wait_send()
         o_local(i).wait()
-    own_g.wait()
+    for i, (rr, yy) in enumerate(((r, y), (r, 1 - y), (1 - r, y), (1 - r, 1 - y))):
+        g_local(i, rr, yy).wait()
     for zt in range(line):
         if zt > 0:
             pl.when(z < zt)(lambda: up_copy(zt, True).wait_send())
@@ -498,7 +550,7 @@
             pl.when(z > zt)(lambda: dn_copy(zt, True).wait_send())
 
 
-def fused(gate_w, up_w, down_w, toks, cots):
+def fused(grad_scale, gate_w, up_w, down_w, toks, cots):
     line = lax.axis_size("fs") // 2
     rows, full = toks.shape
     wrows, width = gate_w.shape[0], gate_w.shape[1] // 4
@@ -511,10 +563,10 @@
     whole = pltpu.VMEM((depth, width), kind)
     unit = pltpu.VMEM((3, rows, cols // 2), kind)
     return pl.pallas_call(
-        functools.partial(fused_kernel, line),
+        functools.partial(fused_kernel, line, grad_scale),
         out_shape=(
             jax.ShapeDtypeStruct((rows, full), kind),
-            jax.ShapeDtypeStruct((wrows, 4 * width), kind),
+            jax.ShapeDtypeStruct((wrows, 4 * width), jnp.float32),
         ),
         in_specs=[anyspec] * 5,
         out_specs=(anyspec,) * 2,
@@ -531,12 +583,14 @@
             pltpu.VMEM((rows, cols), kind),
             whole, whole, whole,
             pltpu.VMEM((2 * wrows, width), kind),
+            pltpu.VMEM((wrows, 4 * width), kind),
+            pltpu.VMEM((wrows, 4 * width), jnp.float32),
             zsem, zsem, zsem, zsem,
             dma((3,)), dma((3,)),
-            dma((6,)), dma((6,)), dma((6,)), dma((6,)), dma((5,)),
+            dma((8,)), dma((8,)), dma((8,)), dma((8,)), dma((5,)),
             dma((4,)), dma((4,)), dma((3,)), dma((3,)), dma((3,)), dma((3,)),
             dma((line,)), dma((line,)), dma((line,)), dma((line,)),
-            dma((3,)), dma((3,)), dma((2,)), dma((2,)), dma((3,)),
+            dma((3,)), dma((3,)), dma((2,)), dma((2,)), dma((2,)), dma((4,)),
         ],
         compiler_params=pltpu.CompilerParams(
             collective_id=1, has_side_effects=True, vmem_limit_bytes=67043328
@@ -758,10 +812,9 @@
     rep_size = lax.axis_size("rep")
     grad_scale = 1.0 / math.sqrt(tok_rows * fs_size * rep_size)
     if lax.axis_size("tp") == 2:
-        grad_input, grad_down = fused(
-            gate_weight, up_weight, down_weight, inputs, cotangent
+        return fused(
+            grad_scale, gate_weight, up_weight, down_weight, inputs, cotangent
         )
-        return (grad_input, grad_down.astype(jnp.float32) * grad_scale)
     contract = (((1,), (1,)), ((), ()))
     contract_tok = (((0,), (0,)), ((), ()))
     width = gate_weight.shape[1] // 4

time: 197 us -> 167 us (0.85)
  the two profiles are of different devices: /device:TPU:8 before, /device:TPU:0 now
where the time goes in v2:
time: 167 us; the launch traced here: 166 us
  Pallas kernels  161 us (96%)
  local copies, waits for them, and re-layouts  4.63 us (3%)
    pallas_call x1, Pallas kernels, fused(): pl.pallas_call(functools.partial(fused_kernel, line, grad_scale), out_sha...  161 us
    unnamed x4, local copies, waits for them, and re-layouts  4.63 us

profile of v2, /device:TPU:0, one launch (start us, length us, event | category | flops | bytes accessed | tf_op | source)
XLA Modules:
  0.0 166.5 jit_solution(4806297963060190542)
XLA Ops:
  0.6 161.2 %fused_all.1 = (bf16[512,2048]{1,0:T(8,128)(2,1)}, f32[256,2048]{1,0:T(8,128)}) custom-call(bf16[256,2048]{1,0:T(8,128)(2,1)} %gate_w.1, bf16[256,2048]{1,0:T(8,128)(2,1)} %up_w.1, bf16[256,2048]{1,0:T(8,128)(2,1)} %down_w.1, bf16[512,2048]{1,0:T(8,128)(2,1)} %toks.1, bf16[512,2048]{1,0:T(8,128)(2,1)} %cots.1), custom_call_target="tpu_custom_call" | custom-call | tf_op jit(solution)/shard_map/fused_all/pallas_call | solution.py:565
  161.8 0.0 copy-start
  161.8 3.3 %copy.9 = bf16[512,2048]{1,0:T(8,128)(2,1)} copy(bf16[512,2048]{1,0:T(8,128)(2,1)} %get-tuple-element.4) | data formatting | bytes 4194304
  165.1 0.0 copy-done
  165.1 1.3 copy.10
Async XLA Ops:
  161.8 3.3 %copy-start = (f32[256,2048]{1,0:T(8,128)S(1)}, f32[256,2048]{1,0:T(8,128)}, u32[]{:S(2)}) copy-start(f32[256,2048]{1,0:T(8,128)} %get-tuple-element.5) | copy-start | bytes 6291460

commit v3 on v2

--- a/solution.py
+++ b/solution.py
@@ -13,9 +13,9 @@
 
 def fused_kernel(
     line, grad_scale, gate_w, up_w, down_w, toks, cots, gi_out, gd_out,
-    x, gu, dn_w, acc, hid, ggu, r1, rx, ry, s3, fin, g, u_in, d_in, gfin, gl, gs,
+    x, gu, dn_w, acc, hid, ggu, r1, rxa, rxb, rya, ryb, s3a, s3b, g, u_in, d_in, gfin, gl,
     up_s, up_r, dn_s, dn_r, wy_s, wy_r, tok_s, tok_r, d2d_s, d2d_r, loc,
-    c_s, c_r, x_s, x_r, yy_s, yy_r, u_s, u_r, d_s, d_r, f_s, f_r, o_s, o_r, out_l, gl_s,
+    c_s, c_r, x_s, x_r, yy_s, yy_r, u_s, u_r, d_s, d_r, f_s, f_r, o_s, o_r,
 ):
     r = lax.axis_index("rep")
     f = lax.axis_index("fs")
@@ -28,7 +28,9 @@
     depth = 2 * line * wrows
     zrows = 2 * wrows
     cols = depth // 2
-    side = cols // 2
+    wide = cols // 2
+    parts_a = rxa.shape[2]
+    parts_b = cols - parts_a
     frows = wrows
     last = line - 2
     has_up, has_dn = z < line - 1, z > 0
@@ -348,8 +350,9 @@
         for sub in range(2):
             settle(d, sub, 2)
     forward(1, dn_w, 2 * width, width, 0, 4)
-    for sub in range(2):
-        forward_end(1, 2, sub)
+    forward_end(1, 2, 0)
+    for up_dir in (True, False):
+        await_recv(up_dir, last, 1, 2)
 
     for i in (0, 3, 5):
         dcopy(i, core).wait_send()
@@ -360,60 +363,120 @@
     its_col = pl.multiple_of((1 - core) * cols, cols)
     part = x.at[0]
 
-    def slopes(row):
-        @pl.loop(0, rows // 32)
+    def slopes(row, count):
+        @pl.loop(0, count // 32)
         def _(i):
             at = pl.ds(pl.multiple_of(row + i * 32, 32), 32)
             grad = acc[at, pl.ds(2 * width, width)]
             ggu[at, pl.ds(0, width)] = (grad * acc[at, pl.ds(0, width)]).astype(ggu.dtype)
             ggu[at, pl.ds(width, width)] = (grad * acc[at, pl.ds(width, width)]).astype(ggu.dtype)
 
-    def back(row, col):
-        @pl.loop(0, cols // side)
+    def back(row, count, col):
+        @pl.loop(0, cols // wide)
         def _(n):
-            at = pl.multiple_of(col + n * side, side)
+            at = pl.multiple_of(col + n * wide, wide)
             one = lax.dot_general(
-                ggu[pl.ds(row, rows), :], gu[pl.ds(at, side), :], (((1,), (1,)), ((), ())),
+                ggu[pl.ds(row, count), :], gu[pl.ds(at, wide), :], (((1,), (1,)), ((), ())),
                 preferred_element_type=jnp.float32,
             )
-            x[0, pl.ds(row, rows), pl.ds(at, side)] = one.astype(x.dtype)
+            x[0, pl.ds(row, count), pl.ds(at, wide)] = one.astype(x.dtype)
+
+    hrows = rows // 2
+    units = [(0, 0, hrows), (0, hrows, hrows), (1, 0, rows), (2, 0, rows), (3, 0, rows)]
+
+    def urow(i):
+        b, at, count = units[i]
+        return pl.multiple_of(slot(*order[b]) + at, hrows)
 
     def core_copy(i):
-        at = pl.ds(slot(*order[i]), rows)
+        at = pl.ds(urow(i), units[i][2])
         return remote(part.at[at, pl.ds(its_col, cols)], r1.at[at, :], c_s.at[i], c_r.at[i], cpart)
 
-    def s1_half(i, second):
-        col = pl.multiple_of(my_col + (side if second else 0), side)
-        return part.at[pl.ds(slot(*order[i]), rows), pl.ds(col, side)]
-
-    def s1(row, second):
-        return (part, row, pl.multiple_of(my_col + (side if second else 0), side), side)
+    first_col = my_col
+    second_col = pl.multiple_of(my_col + parts_a, 128)
+
+    def mine_a(row, count):
+        return part.at[pl.ds(row, count), pl.ds(first_col, parts_a)]
+
+    def mine_b(row, count):
+        return part.at[pl.ds(row, count), pl.ds(second_col, parts_b)]
 
     def x_copy(i):
-        src = s3.at[1] if i == 2 else s1_half(i, False)
-        return remote(src, rx.at[i], x_s.at[i], x_r.at[i], xpart)
+        if i == 3:
+            src, dst = s3b, rxb
+        elif i == 2:
+            src, dst = mine_a(slot(*order[1]), rows), rxa.at[1]
+        else:
+            src, dst = mine_a(urow(i), hrows), rxa.at[0, pl.ds(i * hrows, hrows), :]
+        return remote(src, dst, x_s.at[i], x_r.at[i], xpart)
 
     def y_copy(i):
-        src = s3.at[0] if i == 2 else s1_half((0, 2)[i], True)
-        return remote(src, ry.at[i], yy_s.at[i], yy_r.at[i], ypart)
-
-    for i in range(4):
-        row = slot(*order[i])
-        slopes(row)
-        back(row, its_col)
+        if i == 4:
+            src, dst = s3a, ryb
+        elif i in (2, 3):
+            at = (i - 2) * hrows
+            row = pl.multiple_of(slot(*order[2]) + at, hrows)
+            src, dst = mine_b(row, hrows), rya.at[1, pl.ds(at, hrows), :]
+        else:
+            src, dst = mine_b(urow(i), hrows), rya.at[0, pl.ds(i * hrows, hrows), :]
+        return remote(src, dst, yy_s.at[i], yy_r.at[i], ypart)
+
+    def finish(b):
+        @pl.when(is_end)
+        def _():
+            product(
+                1, slot(*order[b]), (2 * (line - 1 - z) + 1 - y) * wrows, wrows,
+                dn_w, 0, 2 * width, width,
+            )
+
+    def theirs(i):
+        slopes(urow(i), units[i][2])
+        back(urow(i), units[i][2], its_col)
         core_copy(i).start()
-        back(row, my_col)
+
+    def summed(i):
+        back(urow(i), units[i][2], my_col)
         core_copy(i).wait_recv()
-        total((part, row, my_col, cols), [(part, row, my_col, cols), (r1, row, 0, cols)], rows)
-        if i in (0, 1):
-            x_copy(i).start()
-        if i == 0:
-            y_copy(0).start()
-        if i == 2:
-            y_copy(1).start()
-        if i == 2:
-            for t in range(2, line - 1):
-                line_step(t)
+        total(
+            (part, urow(i), my_col, cols),
+            [(part, urow(i), my_col, cols), (r1, urow(i), 0, cols)], units[i][2],
+        )
+
+    finish(0)
+    theirs(0)
+    theirs(1)
+    for i in (0, 1):
+        summed(i)
+        x_copy(i).start()
+        y_copy(i).start()
+    finish(1)
+    theirs(2)
+    summed(2)
+    x_copy(2).start()
+    finish(2)
+    theirs(3)
+    summed(3)
+    y_copy(2).start()
+    for t in range(2, line - 1):
+        line_step(t)
+    finish(3)
+    theirs(4)
+    summed(4)
+
+    for i in (0, 1):
+        x_copy(i).wait_recv()
+    total(
+        (s3a, 0, 0, parts_a),
+        [(part, slot(r, 1 - y), first_col, parts_a), (rxa.at[0], 0, 0, parts_a)], rows,
+    )
+    y_copy(4).start()
+    for i in (0, 1):
+        y_copy(i).wait_recv()
+    total(
+        (s3b, 0, 0, parts_b),
+        [(part, slot(1 - r, y), second_col, parts_b), (rya.at[0], 0, 0, parts_b)], rows,
+    )
+    x_copy(3).start()
 
     zrow = pl.multiple_of(z * zrows, zrows)
 
@@ -455,70 +518,65 @@
             dst = gcols(1 - r, 1 - y) if land else src
         return remote(src, dst, f_s.at[i], f_r.at[i], dev)
 
-    def scaled(i, ref, row, col, rr, yy):
+    def scaled(ref, row, col, rr, yy):
         at_col = gcol(rr, yy)
 
         @pl.loop(0, frows // 64)
         def _(m):
             at = pl.multiple_of(m * 64, 64)
             one = ref[pl.ds(row + at, 64), pl.ds(col, width)].astype(jnp.float32)
-            gs[pl.ds(at, 64), pl.ds(at_col, width)] = one * grad_scale
-
-        g_local(i, rr, yy).start()
-
-    def g_local(i, rr, yy):
-        at = gcol(rr, yy)
-        return pltpu.make_async_copy(
-            gs.at[:, pl.ds(at, width)], gd_out.at[:, pl.ds(at, width)], gl_s.at[i]
-        )
+            gd_out[pl.ds(at, 64), pl.ds(at_col, width)] = one * grad_scale
 
     f_copy(0, False).start()
     f_copy(1, False).start()
-    scaled(0, gfin, pl.multiple_of(y * frows, frows), 0, r, y)
-
-    x_copy(0).wait_recv()
-    total((s3.at[0], 0, 0, side), [s1(slot(r, 1 - y), False), (rx.at[0], 0, 0, side)], rows)
-    y_copy(2).start()
-    y_copy(0).wait_recv()
-    total((s3.at[1], 0, 0, side), [s1(slot(1 - r, y), True), (ry.at[0], 0, 0, side)], rows)
-    x_copy(2).start()
+    y_copy(3).start()
+    scaled(gfin, pl.multiple_of(y * frows, frows), 0, r, y)
+
+    here_row = slot(r, y)
+
+    def o_copy(i, land):
+        base = (1 - core if land else core) * cols
+        if i == 0:
+            at = gi_out.at[:, pl.ds(pl.multiple_of(base, 128), parts_a)]
+        else:
+            at = gi_out.at[
+                pl.ds((i - 1) * hrows, hrows), pl.ds(pl.multiple_of(base + parts_a, 128), parts_b)
+            ]
+        return remote(at, at, o_s.at[i], o_r.at[i], cpart)
+
+    def final_b(at):
+        total(
+            (gi_out, at, second_col, parts_b),
+            [
+                (part, here_row + at, second_col, parts_b),
+                (rya.at[1], at, 0, parts_b), (rxb, at, 0, parts_b),
+            ], hrows,
+        )
+
+    x_copy(2).wait_recv()
+    y_copy(4).wait_recv()
+    total(
+        (gi_out, 0, first_col, parts_a),
+        [
+            (part, here_row, first_col, parts_a),
+            (rxa.at[1], 0, 0, parts_a), (ryb, 0, 0, parts_a),
+        ], rows,
+    )
+    o_copy(0, False).start()
+    x_copy(3).wait_recv()
+    y_copy(2).wait_recv()
+    final_b(0)
+    o_copy(1, False).start()
     f_copy(0, True).wait_recv()
     f_copy(2, False).start()
-    scaled(1, gl, 0, gcol(r, 1 - y), r, 1 - y)
+    scaled(gl, 0, gcol(r, 1 - y), r, 1 - y)
     f_copy(1, True).wait_recv()
-    scaled(2, gl, 0, gcol(1 - r, y), 1 - r, y)
-
-    x_copy(1).wait_recv()
-    y_copy(2).wait_recv()
-    here_row = slot(r, y)
-    total(
-        (fin, 0, 0, side),
-        [s1(here_row, False), (rx.at[1], 0, 0, side), (ry.at[2], 0, 0, side)], rows,
-    )
-
-    def o_copy(i, land):
-        base = (1 - core if land else core) * cols + i * side
-        dst = gi_out.at[:, pl.ds(pl.multiple_of(base, side), side)]
-        return remote(fin.at[:, pl.ds(i * side, side)], dst, o_s.at[i], o_r.at[i], cpart)
-
-    def o_local(i):
-        base = pl.multiple_of(core * cols + i * side, side)
-        return pltpu.make_async_copy(
-            fin.at[:, pl.ds(i * side, side)], gi_out.at[:, pl.ds(base, side)], out_l.at[i]
-        )
-
-    o_copy(0, False).start()
-    o_local(0).start()
-    y_copy(1).wait_recv()
-    x_copy(2).wait_recv()
-    total(
-        (fin, 0, side, side),
-        [s1(here_row, True), (ry.at[1], 0, 0, side), (rx.at[2], 0, 0, side)], rows,
-    )
-    o_copy(1, False).start()
-    o_local(1).start()
+    scaled(gl, 0, gcol(1 - r, y), 1 - r, y)
+    y_copy(3).wait_recv()
+    final_b(hrows)
+    o_copy(2, False).start()
     f_copy(2, True).wait_recv()
-    scaled(3, gl, 0, gcol(1 - r, 1 - y), 1 - r, 1 - y)
+    scaled(gl, 0, gcol(1 - r, 1 - y), 1 - r, 1 - y)
 
     for i in range(ntok):
         if kinds[i] == 1:
@@ -531,18 +589,16 @@
             for sub in range(2):
                 await_send(True, d, sub, k)
                 await_send(False, d, sub, k)
+    for i in range(5):
+        core_copy(i).wait_send()
+        y_copy(i).wait_send()
     for i in range(4):
-        core_copy(i).wait_send()
+        x_copy(i).wait_send()
     for i in range(3):
-        x_copy(i).wait_send()
-        y_copy(i).wait_send()
         f_copy(i, False).wait_send()
-    for i in range(2):
+    for i in range(3):
         o_copy(i, True).wait_recv()
         o_copy(i, False).wait_send()
-        o_local(i).wait()
-    for i, (rr, yy) in enumerate(((r, y), (r, 1 - y), (1 - r, y), (1 - r, 1 - y))):
-        g_local(i, rr, yy).wait()
     for zt in range(line):
         if zt > 0:
             pl.when(z < zt)(lambda: up_copy(zt, True).wait_send())
@@ -561,15 +617,16 @@
     zsem = dma((line - 1, 2, 3))
     anyspec = pl.BlockSpec(memory_space=pl.ANY)
     whole = pltpu.VMEM((depth, width), kind)
-    unit = pltpu.VMEM((3, rows, cols // 2), kind)
+    parts_a = cols * 3 // 8 // 128 * 128
+    parts_b = cols - parts_a
     return pl.pallas_call(
         functools.partial(fused_kernel, line, grad_scale),
         out_shape=(
-            jax.ShapeDtypeStruct((rows, full), kind),
-            jax.ShapeDtypeStruct((wrows, 4 * width), jnp.float32),
+            pltpu.VMEM((rows, full), kind),
+            pltpu.VMEM((wrows, 4 * width), jnp.float32),
         ),
         in_specs=[anyspec] * 5,
-        out_specs=(anyspec,) * 2,
+        out_specs=(pl.BlockSpec(memory_space=pltpu.VMEM),) * 2,
         scratch_shapes=[
             pltpu.VMEM((2, 4 * rows, full), kind),
             pltpu.VMEM((depth, 2 * width), kind),
@@ -578,22 +635,21 @@
             pltpu.VMEM((4 * rows, width), kind),
             pltpu.VMEM((4 * rows, 2 * width), kind),
             pltpu.VMEM((4 * rows, cols), kind),
-            unit, unit,
-            pltpu.VMEM((2, rows, cols // 2), kind),
-            pltpu.VMEM((rows, cols), kind),
+            pltpu.VMEM((2, rows, parts_a), kind), pltpu.VMEM((rows, parts_b), kind),
+            pltpu.VMEM((2, rows, parts_b), kind), pltpu.VMEM((rows, parts_a), kind),
+            pltpu.VMEM((rows, parts_a), kind), pltpu.VMEM((rows, parts_b), kind),
             whole, whole, whole,
             pltpu.VMEM((2 * wrows, width), kind),
             pltpu.VMEM((wrows, 4 * width), kind),
-            pltpu.VMEM((wrows, 4 * width), jnp.float32),
             zsem, zsem, zsem, zsem,
             dma((3,)), dma((3,)),
             dma((8,)), dma((8,)), dma((8,)), dma((8,)), dma((5,)),
-            dma((4,)), dma((4,)), dma((3,)), dma((3,)), dma((3,)), dma((3,)),
+            dma((5,)), dma((5,)), dma((4,)), dma((4,)), dma((5,)), dma((5,)),
             dma((line,)), dma((line,)), dma((line,)), dma((line,)),
-            dma((3,)), dma((3,)), dma((2,)), dma((2,)), dma((2,)), dma((4,)),
+            dma((3,)), dma((3,)), dma((3,)), dma((3,)),
         ],
         compiler_params=pltpu.CompilerParams(
-            collective_id=1, has_side_effects=True, vmem_limit_bytes=67043328
+            collective_id=1, has_side_effects=True, vmem_limit_bytes=59 * 2**20
         ),
         name="fused_all",
     )(gate_w, up_w, down_w, toks, cots)

time: 167 us -> 161 us (0.964)
  Pallas kernels: 161 us -> 157 us
  local copies, waits for them, and re-layouts: 4.63 us -> 2.64 us
    pallas_call x1, Pallas kernels: 161 us -> 157 us  [fused(): pl.pallas_call(functools.partial(fused_kernel, line, grad_scale), out_sha...]
    unnamed x4 -> x2, local copies, waits for them, and re-layouts: 4.63 us -> 2.64 us
where the time goes in v3:
time: 161 us
  Pallas kernels  157 us (98%)
  local copies, waits for them, and re-layouts  2.64 us (2%)
    pallas_call x1, Pallas kernels, fused(): pl.pallas_call(functools.partial(fused_kernel, line, grad_scale), out_sha...  157 us

profile of v3, /device:TPU:0, one launch (start us, length us, event | category | flops | bytes accessed | tf_op | source)
XLA Modules:
  0.0 160.6 jit_solution(10380395117139566636)
XLA Ops:
  0.6 157.4 %fused_all.1 = (bf16[512,2048]{1,0:T(8,128)(2,1)S(1)}, f32[256,2048]{1,0:T(8,128)S(1)}) custom-call(bf16[256,2048]{1,0:T(8,128)(2,1)} %gate_w.1, bf16[256,2048]{1,0:T(8,128)(2,1)} %up_w.1, bf16[256,2048]{1,0:T(8,128)(2,1)} %down_w.1, bf16[512,2048]{1,0:T(8,128)(2,1)} %toks.1, bf16[512,2048]{1,0:T(8,128)(2,1)} %cots.1), custom_call_target="tpu_custom_call" | custom-call | tf_op jit(solution)/shard_map/fused_all/pallas_call | solution.py:622
  158.0 1.3 copy.9
  159.3 1.3 copy.10

commit v4 on v3

--- a/solution.py
+++ b/solution.py
@@ -13,9 +13,9 @@
 
 def fused_kernel(
     line, grad_scale, gate_w, up_w, down_w, toks, cots, gi_out, gd_out,
-    x, gu, dn_w, acc, hid, ggu, r1, rxa, rxb, rya, ryb, s3a, s3b, g, u_in, d_in, gfin, gl,
+    x, gu, dn_w, acc, hid, ggu, r1, rxa, rxb, rya, ryb, s3a, s3b, g, u_in, d_in, gfin, gl, hl,
     up_s, up_r, dn_s, dn_r, wy_s, wy_r, tok_s, tok_r, d2d_s, d2d_r, loc,
-    c_s, c_r, x_s, x_r, yy_s, yy_r, u_s, u_r, d_s, d_r, f_s, f_r, o_s, o_r,
+    c_s, c_r, x_s, x_r, yy_s, yy_r, u_s, u_r, d_s, d_r, f_s, f_r, o_s, o_r, e_s, e_r, h_s, h_r,
 ):
     r = lax.axis_index("rep")
     f = lax.axis_index("fs")
@@ -299,6 +299,9 @@
     for i in (1, 2, 4, 6, 7):
         dcopy(i, 1 - core).wait_recv()
 
+    zrow = pl.multiple_of(z * zrows, zrows)
+    lower = z < line // 2
+
     def block(ref, zt):
         return ref.at[pl.ds(zt * zrows, zrows), :]
 
@@ -308,9 +311,7 @@
     def dn_copy(zt, first):
         return remote(block(g if first else d_in, zt), block(d_in, zt), d_s.at[zt], d_r.at[zt], dn)
 
-    for i in range(line):
-        zt = jnp.where(z < line // 2, line - 1 - i, i)
-
+    def g_block(zt):
         at = pl.multiple_of(zt * zrows, zrows)
         one = lax.dot_general(
             x[1, :, pl.ds(at, zrows)], hid[...], (((0,), (0,)), ((), ())),
@@ -318,46 +319,82 @@
         )
         g[pl.ds(at, zrows), :] = one.astype(g.dtype)
 
-        if i < line - 1:
-            @pl.when(z == 0)
-            def _():
-                up_copy(line - 1 - i, True).start()
-
-            @pl.when(z == line - 1)
-            def _():
-                dn_copy(i, True).start()
+    def gcol(rr, yy):
+        return pl.multiple_of((2 * rr + yy) * width, width)
+
+    def gcols(ref, rr, yy):
+        return ref.at[:, pl.ds(gcol(rr, yy), width)]
+
+    def half_rows(ref, row, yy):
+        return ref.at[pl.ds(pl.multiple_of(row + yy * frows, frows), frows), :]
+
+    def f_copy(i, land, ref=gfin, row=0):
+        if i == 0:
+            src, dst, dev = half_rows(ref, row, 1 - y), gcols(gl, r, 1 - y if land else y), ypart
+        elif i == 1:
+            src, dst, dev = half_rows(ref, row, y), gcols(gl, 1 - r if land else r, y), xpart
+        else:
+            src, dst, dev = gcols(gl, r, 1 - y), gcols(gl, 1 - r if land else r, 1 - y), xpart
+        return remote(src, dst, f_s.at[i], f_r.at[i], dev)
+
+    def e_copy(i, land, ref=gfin, row=0):
+        if i == 0:
+            src, dst, dev = half_rows(ref, row, 1 - y), gcols(hl, r, 1 - y if land else y), ypart
+        else:
+            src, dst, dev = half_rows(ref, row, y), gcols(hl, 1 - r if land else r, y), xpart
+        return remote(src, dst, e_s.at[i], e_r.at[i], dev)
+
+    end_z = jnp.where((z == 1) | (z == line - 1), 0, line - 1)
+    end_dev = {"fs": 2 * end_z + y}
+    next_to_end = (z == 1) | (z == line - 2)
+
+    def h_copy(i, ref=gfin, row=0):
+        rr, yy = ((r, y), (r, 1 - y), (1 - r, y))[i]
+        dst = gcols(hl, rr, yy)
+        src = half_rows(ref, row, y) if i == 0 else dst
+        return remote(src, dst, h_s.at[i], h_r.at[i], end_dev)
+
+    def share(ref, row):
+        h_copy(0, ref, row).start()
+        e_copy(0, False, ref, row).start()
+        e_copy(1, False, ref, row).start()
 
     def line_step(t):
         zt = line - 1 + z - t
-
-        @pl.when((z > 0) & (zt <= line - 1) & (zt > z))
+        row_u = pl.multiple_of(zt * zrows, zrows)
+        is_u = (z > 0) & (zt <= line - 1) & (zt > z)
+        zd = t - (line - 1 - z)
+        row_d = pl.multiple_of(zd * zrows, zrows)
+        is_d = (z < line - 1) & (zd >= 0) & (zd < z)
+        final = t == line - 2
+
+        @pl.when(is_u)
         def _():
             up_copy(zt, False).wait_recv()
-            row = pl.multiple_of(zt * zrows, zrows)
-            total((u_in, row, 0, width), [(g, row, 0, width), (u_in, row, 0, width)], zrows)
+            total((u_in, row_u, 0, width), [(g, row_u, 0, width), (u_in, row_u, 0, width)], zrows)
+
+        @pl.when((is_u & (z < line - 2)) if final else is_u)
+        def _():
             up_copy(zt, False).start()
 
-        zd = t - (line - 1 - z)
-
-        @pl.when((z < line - 1) & (zd >= 0) & (zd < z))
+        @pl.when(is_d)
         def _():
             dn_copy(zd, False).wait_recv()
-            row = pl.multiple_of(zd * zrows, zrows)
-            total((d_in, row, 0, width), [(g, row, 0, width), (d_in, row, 0, width)], zrows)
+            total((d_in, row_d, 0, width), [(g, row_d, 0, width), (d_in, row_d, 0, width)], zrows)
+
+        @pl.when((is_d & (z > 1)) if final else is_d)
+        def _():
             dn_copy(zd, False).start()
 
-    for d in range(last):
-        for sub in range(2):
-            settle(d, sub, 2)
-    forward(1, dn_w, 2 * width, width, 0, 4)
-    forward_end(1, 2, 0)
-    for up_dir in (True, False):
-        await_recv(up_dir, last, 1, 2)
-
-    for i in (0, 3, 5):
-        dcopy(i, core).wait_send()
-    tcopy(5, False).wait_send()
-    line_step(1)
+        if final:
+            @pl.when(z == line - 2)
+            def _():
+                share(u_in, (line - 1) * zrows)
+
+            @pl.when(z == 1)
+            def _():
+                share(d_in, 0)
+
     order = [(1 - r, 1 - y), (1 - r, y), (r, 1 - y), (r, y)]
     my_col = pl.multiple_of(core * cols, cols)
     its_col = pl.multiple_of((1 - core) * cols, cols)
@@ -442,95 +479,23 @@
             [(part, urow(i), my_col, cols), (r1, urow(i), 0, cols)], units[i][2],
         )
 
-    finish(0)
-    theirs(0)
-    theirs(1)
-    for i in (0, 1):
-        summed(i)
-        x_copy(i).start()
-        y_copy(i).start()
-    finish(1)
-    theirs(2)
-    summed(2)
-    x_copy(2).start()
-    finish(2)
-    theirs(3)
-    summed(3)
-    y_copy(2).start()
-    for t in range(2, line - 1):
-        line_step(t)
-    finish(3)
-    theirs(4)
-    summed(4)
-
-    for i in (0, 1):
-        x_copy(i).wait_recv()
-    total(
-        (s3a, 0, 0, parts_a),
-        [(part, slot(r, 1 - y), first_col, parts_a), (rxa.at[0], 0, 0, parts_a)], rows,
-    )
-    y_copy(4).start()
-    for i in (0, 1):
-        y_copy(i).wait_recv()
-    total(
-        (s3b, 0, 0, parts_b),
-        [(part, slot(1 - r, y), second_col, parts_b), (rya.at[0], 0, 0, parts_b)], rows,
-    )
-    x_copy(3).start()
-
-    zrow = pl.multiple_of(z * zrows, zrows)
-
-    def here(ref):
-        return (ref, zrow, 0, width)
-
-    @pl.when(z == 0)
-    def _():
-        dn_copy(0, True).wait_recv()
-        total((gfin, 0, 0, width), [here(g), here(d_in)], zrows)
-
-    @pl.when(z == line - 1)
-    def _():
-        up_copy(line - 1, True).wait_recv()
-        total((gfin, 0, 0, width), [here(g), here(u_in)], zrows)
-
-    @pl.when((z > 0) & (z < line - 1))
-    def _():
-        remote(block(g, z), block(u_in, z), u_s.at[z], u_r.at[z], up).wait_recv()
-        remote(block(g, z), block(d_in, z), d_s.at[z], d_r.at[z], dn).wait_recv()
-        total((gfin, 0, 0, width), [here(g), here(u_in), here(d_in)], zrows)
-
-    def gcol(rr, yy):
-        return pl.multiple_of((2 * rr + yy) * width, width)
-
-    def gcols(rr, yy):
-        return gl.at[:, pl.ds(gcol(rr, yy), width)]
-
-    def grows(yy):
-        return gfin.at[pl.ds(pl.multiple_of(yy * frows, frows), frows), :]
-
-    def f_copy(i, land):
-        if i == 0:
-            src, dst, dev = grows(1 - y), gcols(r, 1 - y) if land else gcols(r, y), ypart
-        elif i == 1:
-            src, dst, dev = grows(y), gcols(1 - r, y) if land else gcols(r, y), xpart
-        else:
-            src, dev = gcols(r, 1 - y), xpart
-            dst = gcols(1 - r, 1 - y) if land else src
-        return remote(src, dst, f_s.at[i], f_r.at[i], dev)
-
-    def scaled(ref, row, col, rr, yy):
-        at_col = gcol(rr, yy)
-
-        @pl.loop(0, frows // 64)
-        def _(m):
-            at = pl.multiple_of(m * 64, 64)
-            one = ref[pl.ds(row + at, 64), pl.ds(col, width)].astype(jnp.float32)
-            gd_out[pl.ds(at, 64), pl.ds(at_col, width)] = one * grad_scale
-
-    f_copy(0, False).start()
-    f_copy(1, False).start()
-    y_copy(3).start()
-    scaled(gfin, pl.multiple_of(y * frows, frows), 0, r, y)
+    def relay_a():
+        for i in (0, 1):
+            x_copy(i).wait_recv()
+        total(
+            (s3a, 0, 0, parts_a),
+            [(part, slot(r, 1 - y), first_col, parts_a), (rxa.at[0], 0, 0, parts_a)], rows,
+        )
+        y_copy(4).start()
+
+    def relay_b():
+        for i in (0, 1):
+            y_copy(i).wait_recv()
+        total(
+            (s3b, 0, 0, parts_b),
+            [(part, slot(1 - r, y), second_col, parts_b), (rya.at[0], 0, 0, parts_b)], rows,
+        )
+        x_copy(3).start()
 
     here_row = slot(r, y)
 
@@ -544,7 +509,23 @@
             ]
         return remote(at, at, o_s.at[i], o_r.at[i], cpart)
 
-    def final_b(at):
+    def final_a():
+        x_copy(2).wait_recv()
+        y_copy(4).wait_recv()
+        total(
+            (gi_out, 0, first_col, parts_a),
+            [
+                (part, here_row, first_col, parts_a),
+                (rxa.at[1], 0, 0, parts_a), (ryb, 0, 0, parts_a),
+            ], rows,
+        )
+        o_copy(0, False).start()
+
+    def final_b(i):
+        at = i * hrows
+        if i == 0:
+            x_copy(3).wait_recv()
+        y_copy(2 + i).wait_recv()
         total(
             (gi_out, at, second_col, parts_b),
             [
@@ -552,31 +533,148 @@
                 (rya.at[1], at, 0, parts_b), (rxb, at, 0, parts_b),
             ], hrows,
         )
-
-    x_copy(2).wait_recv()
-    y_copy(4).wait_recv()
-    total(
-        (gi_out, 0, first_col, parts_a),
-        [
-            (part, here_row, first_col, parts_a),
-            (rxa.at[1], 0, 0, parts_a), (ryb, 0, 0, parts_a),
-        ], rows,
-    )
-    o_copy(0, False).start()
-    x_copy(3).wait_recv()
-    y_copy(2).wait_recv()
-    final_b(0)
-    o_copy(1, False).start()
-    f_copy(0, True).wait_recv()
-    f_copy(2, False).start()
-    scaled(gl, 0, gcol(r, 1 - y), r, 1 - y)
-    f_copy(1, True).wait_recv()
-    scaled(gl, 0, gcol(1 - r, y), 1 - r, y)
-    y_copy(3).wait_recv()
-    final_b(hrows)
-    o_copy(2, False).start()
-    f_copy(2, True).wait_recv()
-    scaled(gl, 0, gcol(1 - r, 1 - y), 1 - r, 1 - y)
+        o_copy(1 + i, False).start()
+
+    def scaled(terms, rr, yy, keep=None):
+        at_col = gcol(rr, yy)
+
+        @pl.loop(0, frows // 64)
+        def _(m):
+            at = pl.multiple_of(m * 64, 64)
+            value = None
+            for ref, row, col in terms:
+                one = ref[pl.ds(row + at, 64), pl.ds(col, width)].astype(jnp.float32)
+                value = one if value is None else value + one
+            if keep is not None:
+                keep[pl.ds(at, 64), pl.ds(at_col, width)] = value.astype(keep.dtype)
+            gd_out[pl.ds(at, 64), pl.ds(at_col, width)] = value * grad_scale
+
+    def inputs_sent():
+        for i in (0, 3, 5):
+            dcopy(i, core).wait_send()
+        tcopy(5, False).wait_send()
+
+    @pl.when(is_end)
+    def _():
+        for i in range(line):
+            g_block(jnp.where(lower, line - 1 - i, i))
+            if i < line - 1:
+                @pl.when(lower)
+                def _():
+                    up_copy(line - 1 - i, True).start()
+
+                @pl.when(jnp.logical_not(lower))
+                def _():
+                    dn_copy(i, True).start()
+        f_copy(0, False, g, zrow).start()
+        f_copy(1, False, g, zrow).start()
+        for d in range(last):
+            for sub in range(2):
+                settle(d, sub, 2)
+        forward(1, dn_w, 2 * width, width, 0, 4)
+        forward_end(1, 2, 0)
+        for up_dir in (True, False):
+            await_recv(up_dir, last, 1, 2)
+        inputs_sent()
+        finish(0)
+        theirs(0)
+        theirs(1)
+        for i in (0, 1):
+            summed(i)
+            x_copy(i).start()
+            y_copy(i).start()
+        finish(1)
+        theirs(2)
+        summed(2)
+        x_copy(2).start()
+        finish(2)
+        theirs(3)
+        summed(3)
+        y_copy(2).start()
+        finish(3)
+        theirs(4)
+        summed(4)
+        relay_a()
+        y_copy(3).start()
+        relay_b()
+        f_copy(0, True).wait_recv()
+        h_copy(1).wait_recv()
+        scaled([(gl, 0, gcol(r, 1 - y)), (hl, 0, gcol(r, 1 - y))], r, 1 - y, gl)
+        f_copy(2, False).start()
+        h_copy(0).wait_recv()
+        scaled([(g, pl.multiple_of(zrow + y * frows, frows), 0), (hl, 0, gcol(r, y))], r, y)
+        final_a()
+        final_b(0)
+        f_copy(1, True).wait_recv()
+        h_copy(2).wait_recv()
+        scaled([(gl, 0, gcol(1 - r, y)), (hl, 0, gcol(1 - r, y))], 1 - r, y)
+        final_b(1)
+        f_copy(2, True).wait_recv()
+        scaled([(gl, 0, gcol(1 - r, 1 - y))], 1 - r, 1 - y)
+
+    @pl.when(jnp.logical_not(is_end))
+    def _():
+        inputs_sent()
+        forward(1, dn_w, 2 * width, width, 3, 1)
+        theirs(0)
+        theirs(1)
+        for i in (0, 1):
+            summed(i)
+            x_copy(i).start()
+            y_copy(i).start()
+        g_block(jnp.where(lower, line - 1, 0))
+        forward(1, dn_w, 2 * width, width, 1, 1)
+        theirs(2)
+        summed(2)
+        x_copy(2).start()
+        line_step(1)
+        forward(1, dn_w, 2 * width, width, 2, 1)
+        theirs(3)
+        summed(3)
+        y_copy(2).start()
+        relay_a()
+        relay_b()
+        for i in range(1, line):
+            g_block(jnp.where(lower, line - 1 - i, i))
+        for t in range(2, line - 1):
+            line_step(t)
+        forward(1, dn_w, 2 * width, width, 0, 1)
+        theirs(4)
+        summed(4)
+        up_copy(z, False).wait_recv()
+        dn_copy(z, False).wait_recv()
+        total(
+            (gfin, 0, 0, width),
+            [(g, zrow, 0, width), (u_in, zrow, 0, width), (d_in, zrow, 0, width)], zrows,
+        )
+        f_copy(0, False).start()
+        f_copy(1, False).start()
+        y_copy(3).start()
+        scaled([(gfin, pl.multiple_of(y * frows, frows), 0)], r, y)
+        final_a()
+        final_b(0)
+
+        @pl.when(next_to_end)
+        def _():
+            for i in (0, 1):
+                e_copy(i, True).wait_recv()
+                h_copy(1 + i).start()
+
+        f_copy(0, True).wait_recv()
+        f_copy(2, False).start()
+        scaled([(gl, 0, gcol(r, 1 - y))], r, 1 - y)
+        f_copy(1, True).wait_recv()
+        scaled([(gl, 0, gcol(1 - r, y))], 1 - r, y)
+        final_b(1)
+        f_copy(2, True).wait_recv()
+        scaled([(gl, 0, gcol(1 - r, 1 - y))], 1 - r, 1 - y)
+
+        @pl.when(next_to_end)
+        def _():
+            for i in (0, 1):
+                e_copy(i, False).wait_send()
+            for i in (0, 1, 2):
+                h_copy(i).wait_send()
 
     for i in range(ntok):
         if kinds[i] == 1:
@@ -601,9 +699,11 @@
         o_copy(i, False).wait_send()
     for zt in range(line):
         if zt > 0:
-            pl.when(z < zt)(lambda: up_copy(zt, True).wait_send())
+            far = line - 2 if zt == line - 1 else zt
+            pl.when(z < far)(lambda: up_copy(zt, True).wait_send())
         if zt < line - 1:
-            pl.when(z > zt)(lambda: dn_copy(zt, True).wait_send())
+            near = 1 if zt == 0 else zt
+            pl.when(z > near)(lambda: dn_copy(zt, True).wait_send())
 
 
 def fused(grad_scale, gate_w, up_w, down_w, toks, cots):
@@ -641,12 +741,14 @@
             whole, whole, whole,
             pltpu.VMEM((2 * wrows, width), kind),
             pltpu.VMEM((wrows, 4 * width), kind),
+            pltpu.VMEM((wrows, 4 * width), kind),
             zsem, zsem, zsem, zsem,
             dma((3,)), dma((3,)),
             dma((8,)), dma((8,)), dma((8,)), dma((8,)), dma((5,)),
             dma((5,)), dma((5,)), dma((4,)), dma((4,)), dma((5,)), dma((5,)),
             dma((line,)), dma((line,)), dma((line,)), dma((line,)),
             dma((3,)), dma((3,)), dma((3,)), dma((3,)),
+            dma((2,)), dma((2,)), dma((3,)), dma((3,)),
         ],
         compiler_params=pltpu.CompilerParams(
             collective_id=1, has_side_effects=True, vmem_limit_bytes=59 * 2**20
@@ -867,7 +969,7 @@
     fs_size = lax.axis_size("fs")
     rep_size = lax.axis_size("rep")
     grad_scale = 1.0 / math.sqrt(tok_rows * fs_size * rep_size)
-    if lax.axis_size("tp") == 2:
+    if lax.axis_size("tp") == 2 and rep_size == 2 and fs_size >= 8:
         return fused(
             grad_scale, gate_weight, up_weight, down_weight, inputs, cotangent
         )

time: 161 us -> 155 us (0.963)
  Pallas kernels: 157 us -> 152 us
    pallas_call x1, Pallas kernels: 157 us -> 152 us  [fused(): pl.pallas_call(functools.partial(fused_kernel, line, grad_scale), out_sha...]
where the time goes in v4:
time: 155 us
  Pallas kernels  152 us (98%)
  local copies, waits for them, and re-layouts  2.64 us (2%)
    pallas_call x1, Pallas kernels, fused(): pl.pallas_call(functools.partial(fused_kernel, line, grad_scale), out_sha...  152 us

profile of v4, /device:TPU:0, one launch (start us, length us, event | category | flops | bytes accessed | tf_op | source)
XLA Modules:
  0.0 155.1 jit_solution(16735078835083166195)
XLA Ops:
  0.6 151.8 %fused_all.1 = (bf16[512,2048]{1,0:T(8,128)(2,1)S(1)}, f32[256,2048]{1,0:T(8,128)S(1)}) custom-call(bf16[256,2048]{1,0:T(8,128)(2,1)} %gate_w.1, bf16[256,2048]{1,0:T(8,128)(2,1)} %up_w.1, bf16[256,2048]{1,0:T(8,128)(2,1)} %down_w.1, bf16[512,2048]{1,0:T(8,128)(2,1)} %toks.1, bf16[512,2048]{1,0:T(8,128)(2,1)} %cots.1), custom_call_target="tpu_custom_call" | custom-call | tf_op jit(solution)/shard_map/fused_all/pallas_call | solution.py:722
  152.5 1.3 copy.9
  153.8 1.3 copy.10

commit v5 on v4

--- a/solution.py
+++ b/solution.py
@@ -12,7 +12,7 @@
 
 
 def fused_kernel(
-    line, grad_scale, gate_w, up_w, down_w, toks, cots, gi_out, gd_out,
+    line, grad_scale, end_a, mid_a, gate_w, up_w, down_w, toks, cots, gi_out, gd_out,
     x, gu, dn_w, acc, hid, ggu, r1, rxa, rxb, rya, ryb, s3a, s3b, g, u_in, d_in, gfin, gl, hl,
     up_s, up_r, dn_s, dn_r, wy_s, wy_r, tok_s, tok_r, d2d_s, d2d_r, loc,
     c_s, c_r, x_s, x_r, yy_s, yy_r, u_s, u_r, d_s, d_r, f_s, f_r, o_s, o_r, e_s, e_r, h_s, h_r,
@@ -29,8 +29,6 @@
     zrows = 2 * wrows
     cols = depth // 2
     wide = cols // 2
-    parts_a = rxa.shape[2]
-    parts_b = cols - parts_a
     frows = wrows
     last = line - 2
     has_up, has_dn = z < line - 1, z > 0
@@ -340,8 +338,10 @@
     def e_copy(i, land, ref=gfin, row=0):
         if i == 0:
             src, dst, dev = half_rows(ref, row, 1 - y), gcols(hl, r, 1 - y if land else y), ypart
+        elif i == 1:
+            src, dst, dev = half_rows(ref, row, y), gcols(hl, 1 - r if land else r, y), xpart
         else:
-            src, dst, dev = half_rows(ref, row, y), gcols(hl, 1 - r if land else r, y), xpart
+            src, dst, dev = gcols(hl, r, 1 - y), gcols(hl, 1 - r if land else r, 1 - y), xpart
         return remote(src, dst, e_s.at[i], e_r.at[i], dev)
 
     end_z = jnp.where((z == 1) | (z == line - 1), 0, line - 1)
@@ -349,7 +349,7 @@
     next_to_end = (z == 1) | (z == line - 2)
 
     def h_copy(i, ref=gfin, row=0):
-        rr, yy = ((r, y), (r, 1 - y), (1 - r, y))[i]
+        rr, yy = ((r, y), (r, 1 - y), (1 - r, y), (1 - r, 1 - y))[i]
         dst = gcols(hl, rr, yy)
         src = half_rows(ref, row, y) if i == 0 else dst
         return remote(src, dst, h_s.at[i], h_r.at[i], end_dev)
@@ -429,35 +429,6 @@
         at = pl.ds(urow(i), units[i][2])
         return remote(part.at[at, pl.ds(its_col, cols)], r1.at[at, :], c_s.at[i], c_r.at[i], cpart)
 
-    first_col = my_col
-    second_col = pl.multiple_of(my_col + parts_a, 128)
-
-    def mine_a(row, count):
-        return part.at[pl.ds(row, count), pl.ds(first_col, parts_a)]
-
-    def mine_b(row, count):
-        return part.at[pl.ds(row, count), pl.ds(second_col, parts_b)]
-
-    def x_copy(i):
-        if i == 3:
-            src, dst = s3b, rxb
-        elif i == 2:
-            src, dst = mine_a(slot(*order[1]), rows), rxa.at[1]
-        else:
-            src, dst = mine_a(urow(i), hrows), rxa.at[0, pl.ds(i * hrows, hrows), :]
-        return remote(src, dst, x_s.at[i], x_r.at[i], xpart)
-
-    def y_copy(i):
-        if i == 4:
-            src, dst = s3a, ryb
-        elif i in (2, 3):
-            at = (i - 2) * hrows
-            row = pl.multiple_of(slot(*order[2]) + at, hrows)
-            src, dst = mine_b(row, hrows), rya.at[1, pl.ds(at, hrows), :]
-        else:
-            src, dst = mine_b(urow(i), hrows), rya.at[0, pl.ds(i * hrows, hrows), :]
-        return remote(src, dst, yy_s.at[i], yy_r.at[i], ypart)
-
     def finish(b):
         @pl.when(is_end)
         def _():
@@ -479,63 +450,104 @@
             [(part, urow(i), my_col, cols), (r1, urow(i), 0, cols)], units[i][2],
         )
 
-    def relay_a():
-        for i in (0, 1):
-            x_copy(i).wait_recv()
-        total(
-            (s3a, 0, 0, parts_a),
-            [(part, slot(r, 1 - y), first_col, parts_a), (rxa.at[0], 0, 0, parts_a)], rows,
-        )
-        y_copy(4).start()
-
-    def relay_b():
-        for i in (0, 1):
-            y_copy(i).wait_recv()
-        total(
-            (s3b, 0, 0, parts_b),
-            [(part, slot(1 - r, y), second_col, parts_b), (rya.at[0], 0, 0, parts_b)], rows,
-        )
-        x_copy(3).start()
-
     here_row = slot(r, y)
 
-    def o_copy(i, land):
-        base = (1 - core if land else core) * cols
-        if i == 0:
-            at = gi_out.at[:, pl.ds(pl.multiple_of(base, 128), parts_a)]
-        else:
-            at = gi_out.at[
-                pl.ds((i - 1) * hrows, hrows), pl.ds(pl.multiple_of(base + parts_a, 128), parts_b)
-            ]
-        return remote(at, at, o_s.at[i], o_r.at[i], cpart)
-
-    def final_a():
-        x_copy(2).wait_recv()
-        y_copy(4).wait_recv()
-        total(
-            (gi_out, 0, first_col, parts_a),
-            [
-                (part, here_row, first_col, parts_a),
-                (rxa.at[1], 0, 0, parts_a), (ryb, 0, 0, parts_a),
-            ], rows,
-        )
-        o_copy(0, False).start()
-
-    def final_b(i):
-        at = i * hrows
-        if i == 0:
-            x_copy(3).wait_recv()
-        y_copy(2 + i).wait_recv()
-        total(
-            (gi_out, at, second_col, parts_b),
-            [
-                (part, here_row + at, second_col, parts_b),
-                (rya.at[1], at, 0, parts_b), (rxb, at, 0, parts_b),
-            ], hrows,
-        )
-        o_copy(1 + i, False).start()
-
-    def scaled(terms, rr, yy, keep=None):
+    def plane_sums(pa):
+        pb = cols - pa
+        second_col = pl.multiple_of(my_col + pa, 128)
+
+        def mine_a(row, count):
+            return part.at[pl.ds(row, count), pl.ds(my_col, pa)]
+
+        def mine_b(row, count):
+            return part.at[pl.ds(row, count), pl.ds(second_col, pb)]
+
+        def x_copy(i):
+            if i == 3:
+                src, dst = s3b.at[:, pl.ds(0, pb)], rxb.at[:, pl.ds(0, pb)]
+            elif i == 2:
+                src, dst = mine_a(slot(*order[1]), rows), rxa.at[1, :, pl.ds(0, pa)]
+            else:
+                src, dst = mine_a(urow(i), hrows), rxa.at[0, pl.ds(i * hrows, hrows), pl.ds(0, pa)]
+            return remote(src, dst, x_s.at[i], x_r.at[i], xpart)
+
+        def y_copy(i):
+            if i == 4:
+                src, dst = s3a.at[:, pl.ds(0, pa)], ryb.at[:, pl.ds(0, pa)]
+            elif i in (2, 3):
+                at = (i - 2) * hrows
+                row = pl.multiple_of(slot(*order[2]) + at, hrows)
+                src, dst = mine_b(row, hrows), rya.at[1, pl.ds(at, hrows), pl.ds(0, pb)]
+            else:
+                src, dst = mine_b(urow(i), hrows), rya.at[0, pl.ds(i * hrows, hrows), pl.ds(0, pb)]
+            return remote(src, dst, yy_s.at[i], yy_r.at[i], ypart)
+
+        def relay_a():
+            for i in (0, 1):
+                x_copy(i).wait_recv()
+            total(
+                (s3a, 0, 0, pa),
+                [(part, slot(r, 1 - y), my_col, pa), (rxa.at[0], 0, 0, pa)], rows,
+            )
+            y_copy(4).start()
+
+        def relay_b():
+            for i in (0, 1):
+                y_copy(i).wait_recv()
+            total(
+                (s3b, 0, 0, pb),
+                [(part, slot(1 - r, y), second_col, pb), (rya.at[0], 0, 0, pb)], rows,
+            )
+            x_copy(3).start()
+
+        def o_copy(i, land):
+            base = (1 - core if land else core) * cols
+            if i == 0:
+                at = gi_out.at[:, pl.ds(pl.multiple_of(base, 128), pa)]
+            else:
+                at = gi_out.at[
+                    pl.ds((i - 1) * hrows, hrows), pl.ds(pl.multiple_of(base + pa, 128), pb)
+                ]
+            return remote(at, at, o_s.at[i], o_r.at[i], cpart)
+
+        def final_a():
+            x_copy(2).wait_recv()
+            y_copy(4).wait_recv()
+            total(
+                (gi_out, 0, my_col, pa),
+                [
+                    (part, here_row, my_col, pa),
+                    (rxa.at[1], 0, 0, pa), (ryb, 0, 0, pa),
+                ], rows,
+            )
+            o_copy(0, False).start()
+
+        def final_b(i):
+            at = i * hrows
+            if i == 0:
+                x_copy(3).wait_recv()
+            y_copy(2 + i).wait_recv()
+            total(
+                (gi_out, at, second_col, pb),
+                [
+                    (part, here_row + at, second_col, pb),
+                    (rya.at[1], at, 0, pb), (rxb, at, 0, pb),
+                ], hrows,
+            )
+            o_copy(1 + i, False).start()
+
+        def settled():
+            for i in range(5):
+                y_copy(i).wait_send()
+            for i in range(4):
+                x_copy(i).wait_send()
+            for i in range(3):
+                o_copy(i, True).wait_recv()
+                o_copy(i, False).wait_send()
+
+        return x_copy, y_copy, relay_a, relay_b, final_a, final_b, settled
+
+    def scaled(terms, rr, yy):
         at_col = gcol(rr, yy)
 
         @pl.loop(0, frows // 64)
@@ -545,8 +557,6 @@
             for ref, row, col in terms:
                 one = ref[pl.ds(row + at, 64), pl.ds(col, width)].astype(jnp.float32)
                 value = one if value is None else value + one
-            if keep is not None:
-                keep[pl.ds(at, 64), pl.ds(at_col, width)] = value.astype(keep.dtype)
             gd_out[pl.ds(at, 64), pl.ds(at_col, width)] = value * grad_scale
 
     def inputs_sent():
@@ -556,6 +566,7 @@
 
     @pl.when(is_end)
     def _():
+        x_copy, y_copy, relay_a, relay_b, final_a, final_b, settled = plane_sums(end_a)
         for i in range(line):
             g_block(jnp.where(lower, line - 1 - i, i))
             if i < line - 1:
@@ -572,6 +583,8 @@
             for sub in range(2):
                 settle(d, sub, 2)
         forward(1, dn_w, 2 * width, width, 0, 4)
+        f_copy(0, True).wait_recv()
+        f_copy(2, False).start()
         forward_end(1, 2, 0)
         for up_dir in (True, False):
             await_recv(up_dir, last, 1, 2)
@@ -597,23 +610,25 @@
         relay_a()
         y_copy(3).start()
         relay_b()
-        f_copy(0, True).wait_recv()
-        h_copy(1).wait_recv()
-        scaled([(gl, 0, gcol(r, 1 - y)), (hl, 0, gcol(r, 1 - y))], r, 1 - y, gl)
-        f_copy(2, False).start()
         h_copy(0).wait_recv()
         scaled([(g, pl.multiple_of(zrow + y * frows, frows), 0), (hl, 0, gcol(r, y))], r, y)
         final_a()
         final_b(0)
-        f_copy(1, True).wait_recv()
-        h_copy(2).wait_recv()
-        scaled([(gl, 0, gcol(1 - r, y)), (hl, 0, gcol(1 - r, y))], 1 - r, y)
+        for i, (rr, yy) in enumerate(((r, 1 - y), (1 - r, y))):
+            if i == 1:
+                f_copy(1, True).wait_recv()
+            h_copy(1 + i).wait_recv()
+            scaled([(gl, 0, gcol(rr, yy)), (hl, 0, gcol(rr, yy))], rr, yy)
         final_b(1)
         f_copy(2, True).wait_recv()
-        scaled([(gl, 0, gcol(1 - r, 1 - y))], 1 - r, 1 - y)
+        h_copy(3).wait_recv()
+        diag = gcol(1 - r, 1 - y)
+        scaled([(gl, 0, diag), (hl, 0, diag)], 1 - r, 1 - y)
+        settled()
 
     @pl.when(jnp.logical_not(is_end))
     def _():
+        x_copy, y_copy, relay_a, relay_b, final_a, final_b, settled = plane_sums(mid_a)
         inputs_sent()
         forward(1, dn_w, 2 * width, width, 3, 1)
         theirs(0)
@@ -648,17 +663,25 @@
             [(g, zrow, 0, width), (u_in, zrow, 0, width), (d_in, zrow, 0, width)], zrows,
         )
         f_copy(0, False).start()
-        f_copy(1, False).start()
         y_copy(3).start()
         scaled([(gfin, pl.multiple_of(y * frows, frows), 0)], r, y)
+
+        @pl.when(next_to_end)
+        def _():
+            e_copy(0, True).wait_recv()
+            e_copy(2, False).start()
+            h_copy(1).start()
+            e_copy(1, True).wait_recv()
+            h_copy(2).start()
+
+        f_copy(1, False).start()
         final_a()
         final_b(0)
 
         @pl.when(next_to_end)
         def _():
-            for i in (0, 1):
-                e_copy(i, True).wait_recv()
-                h_copy(1 + i).start()
+            e_copy(2, True).wait_recv()
+            h_copy(3).start()
 
         f_copy(0, True).wait_recv()
         f_copy(2, False).start()
@@ -671,10 +694,12 @@
 
         @pl.when(next_to_end)
         def _():
-            for i in (0, 1):
+            for i in range(3):
                 e_copy(i, False).wait_send()
-            for i in (0, 1, 2):
+            for i in range(4):
                 h_copy(i).wait_send()
+
+        settled()
 
     for i in range(ntok):
         if kinds[i] == 1:
@@ -689,14 +714,8 @@
                 await_send(False, d, sub, k)
     for i in range(5):
         core_copy(i).wait_send()
-        y_copy(i).wait_send()
-    for i in range(4):
-        x_copy(i).wait_send()
     for i in range(3):
         f_copy(i, False).wait_send()
-    for i in range(3):
-        o_copy(i, True).wait_recv()
-        o_copy(i, False).wait_send()
     for zt in range(line):
         if zt > 0:
             far = line - 2 if zt == line - 1 else zt
@@ -717,10 +736,10 @@
     zsem = dma((line - 1, 2, 3))
     anyspec = pl.BlockSpec(memory_space=pl.ANY)
     whole = pltpu.VMEM((depth, width), kind)
-    parts_a = cols * 3 // 8 // 128 * 128
-    parts_b = cols - parts_a
+    end_a, mid_a = cols // 2, cols // 4
+    most_b = cols - mid_a
     return pl.pallas_call(
-        functools.partial(fused_kernel, line, grad_scale),
+        functools.partial(fused_kernel, line, grad_scale, end_a, mid_a),
         out_shape=(
             pltpu.VMEM((rows, full), kind),
             pltpu.VMEM((wrows, 4 * width), jnp.float32),
@@ -735,9 +754,9 @@
             pltpu.VMEM((4 * rows, width), kind),
             pltpu.VMEM((4 * rows, 2 * width), kind),
             pltpu.VMEM((4 * rows, cols), kind),
-            pltpu.VMEM((2, rows, parts_a), kind), pltpu.VMEM((rows, parts_b), kind),
-            pltpu.VMEM((2, rows, parts_b), kind), pltpu.VMEM((rows, parts_a), kind),
-            pltpu.VMEM((rows, parts_a), kind), pltpu.VMEM((rows, parts_b), kind),
+            pltpu.VMEM((2, rows, end_a), kind), pltpu.VMEM((rows, most_b), kind),
+            pltpu.VMEM((2, rows, most_b), kind), pltpu.VMEM((rows, end_a), kind),
+            pltpu.VMEM((rows, end_a), kind), pltpu.VMEM((rows, most_b), kind),
             whole, whole, whole,
             pltpu.VMEM((2 * wrows, width), kind),
             pltpu.VMEM((wrows, 4 * width), kind),
@@ -748,7 +767,7 @@
             dma((5,)), dma((5,)), dma((4,)), dma((4,)), dma((5,)), dma((5,)),
             dma((line,)), dma((line,)), dma((line,)), dma((line,)),
             dma((3,)), dma((3,)), dma((3,)), dma((3,)),
-            dma((2,)), dma((2,)), dma((3,)), dma((3,)),
+            dma((3,)), dma((3,)), dma((4,)), dma((4,)),
         ],
         compiler_params=pltpu.CompilerParams(
             collective_id=1, has_side_effects=True, vmem_limit_bytes=59 * 2**20

time: 155 us -> 155 us (level)
  Pallas kernels: 152 us -> 150 us
where the time goes in v5:
time: 155 us; the launch traced here: 154 us
  Pallas kernels  150 us (97%)
  local copies, waits for them, and re-layouts  2.64 us (2%)
    pallas_call x1, Pallas kernels, fused(): pl.pallas_call(functools.partial(fused_kernel, line, grad_scale, end_a, m...  150 us

profile of v5, /device:TPU:0, one launch (start us, length us, event | category | flops | bytes accessed | tf_op | source)
XLA Modules:
  0.0 153.6 jit_solution(17336078747905458613)
XLA Ops:
  0.6 150.3 %fused_all.1 = (bf16[512,2048]{1,0:T(8,128)(2,1)S(1)}, f32[256,2048]{1,0:T(8,128)S(1)}) custom-call(bf16[256,2048]{1,0:T(8,128)(2,1)} %gate_w.1, bf16[256,2048]{1,0:T(8,128)(2,1)} %up_w.1, bf16[256,2048]{1,0:T(8,128)(2,1)} %down_w.1, bf16[512,2048]{1,0:T(8,128)(2,1)} %toks.1, bf16[512,2048]{1,0:T(8,128)(2,1)} %cots.1), custom_call_target="tpu_custom_call" | custom-call | tf_op jit(solution)/shard_map/fused_all/pallas_call | solution.py:741
  151.0 1.3 copy.9
  152.3 1.3 copy.10

commit v6 on v5

--- a/solution.py
+++ b/solution.py
@@ -736,7 +736,7 @@
     zsem = dma((line - 1, 2, 3))
     anyspec = pl.BlockSpec(memory_space=pl.ANY)
     whole = pltpu.VMEM((depth, width), kind)
-    end_a, mid_a = cols // 2, cols // 4
+    end_a, mid_a = cols // 2, cols * 3 // 8 // 128 * 128
     most_b = cols - mid_a
     return pl.pallas_call(
         functools.partial(fused_kernel, line, grad_scale, end_a, mid_a),
@@ -776,6 +776,32 @@
     )(gate_w, up_w, down_w, toks, cots)
 
 
+def place_kernel(a, b, a_out, b_out, sems):
+    copies = [
+        pltpu.make_async_copy(a, a_out, sems.at[0]),
+        pltpu.make_async_copy(b, b_out, sems.at[1]),
+    ]
+    for copy in copies:
+        copy.start()
+    for copy in copies:
+        copy.wait()
+
+
+def place(a, b):
+    anyspec = pl.BlockSpec(memory_space=pl.ANY)
+    return pl.pallas_call(
+        place_kernel,
+        out_shape=(
+            jax.ShapeDtypeStruct(a.shape, a.dtype), jax.ShapeDtypeStruct(b.shape, b.dtype),
+        ),
+        in_specs=[pl.BlockSpec(memory_space=pltpu.VMEM)] * 2,
+        out_specs=(anyspec,) * 2,
+        scratch_shapes=[pltpu.SemaphoreType.DMA((2,))],
+        compiler_params=pltpu.CompilerParams(vmem_limit_bytes=16 * 2**20),
+        name="place",
+    )(a, b)
+
+
 def gather_kernel(
     line, units, gate_w, up_w, down_w, toks, cots, gu_out, d_out, t_out, w_tmp, t_tmp,
     up_s, up_r, dn_s, dn_r, y_s, y_r, tok_s, tok_r, d2d_s, d2d_r, loc, loc2,
@@ -989,9 +1015,9 @@
     rep_size = lax.axis_size("rep")
     grad_scale = 1.0 / math.sqrt(tok_rows * fs_size * rep_size)
     if lax.axis_size("tp") == 2 and rep_size == 2 and fs_size >= 8:
-        return fused(
+        return place(*fused(
             grad_scale, gate_weight, up_weight, down_weight, inputs, cotangent
-        )
+        ))
     contract = (((1,), (1,)), ((), ()))
     contract_tok = (((0,), (0,)), ((), ()))
     width = gate_weight.shape[1] // 4

time: 155 us -> 154 us (level)
  Pallas kernels: 150 us -> 153 us
  local copies, waits for them, and re-layouts: 2.64 us -> 0 us
    unnamed x2 -> x0, local copies, waits for them, and re-layouts: 2.64 us -> none
    pallas_call x0 -> x1, Pallas kernels: none -> 2.03 us  [place(): pl.pallas_call(place_kernel, out_shape=(jax.ShapeDtypeStruct(a.shape, a.d...]
where the time goes in v6:
time: 154 us
  Pallas kernels  153 us (99%)
    pallas_call x1, Pallas kernels, fused(): pl.pallas_call(functools.partial(fused_kernel, line, grad_scale, end_a, m...  151 us

profile of v6, /device:TPU:0, one launch (start us, length us, event | category | flops | bytes accessed | tf_op | source)
XLA Modules:
  0.0 153.7 jit_solution(6673389455219349890)
XLA Ops:
  0.6 150.9 %fused_all.1 = (bf16[512,2048]{1,0:T(8,128)(2,1)S(1)}, f32[256,2048]{1,0:T(8,128)S(1)}) custom-call(bf16[256,2048]{1,0:T(8,128)(2,1)} %gate_w.1, bf16[256,2048]{1,0:T(8,128)(2,1)} %up_w.1, bf16[256,2048]{1,0:T(8,128)(2,1)} %down_w.1, bf16[512,2048]{1,0:T(8,128)(2,1)} %toks.1, bf16[512,2048]{1,0:T(8,128)(2,1)} %cots.1), custom_call_target="tpu_custom_call" | custom-call | tf_op jit(solution)/shard_map/fused_all/pallas_call | solution.py:741
  151.5 2.0 %place.1 = (bf16[512,2048]{1,0:T(8,128)(2,1)}, f32[256,2048]{1,0:T(8,128)}) custom-call(bf16[512,2048]{1,0:T(8,128)(2,1)S(1)} %get-tuple-element.4.a, f32[256,2048]{1,0:T(8,128)S(1)} %get-tuple-element.5.b), custom_call_target="tpu_custom_call" | custom-call | tf_op jit(solution)/shard_map/place/pallas_call | solution.py:792

commit v7 on v6

--- a/solution.py
+++ b/solution.py
@@ -408,26 +408,19 @@
             ggu[at, pl.ds(0, width)] = (grad * acc[at, pl.ds(0, width)]).astype(ggu.dtype)
             ggu[at, pl.ds(width, width)] = (grad * acc[at, pl.ds(width, width)]).astype(ggu.dtype)
 
-    def back(row, count, col):
-        @pl.loop(0, cols // wide)
-        def _(n):
-            at = pl.multiple_of(col + n * wide, wide)
+    def back(row, count, col, n):
+        step = min(n, wide) if n % wide == 0 else n
+
+        @pl.loop(0, n // step)
+        def _(i):
+            at = pl.multiple_of(col + i * step, 128)
             one = lax.dot_general(
-                ggu[pl.ds(row, count), :], gu[pl.ds(at, wide), :], (((1,), (1,)), ((), ())),
+                ggu[pl.ds(row, count), :], gu[pl.ds(at, step), :], (((1,), (1,)), ((), ())),
                 preferred_element_type=jnp.float32,
             )
-            x[0, pl.ds(row, count), pl.ds(at, wide)] = one.astype(x.dtype)
+            x[0, pl.ds(row, count), pl.ds(at, step)] = one.astype(x.dtype)
 
     hrows = rows // 2
-    units = [(0, 0, hrows), (0, hrows, hrows), (1, 0, rows), (2, 0, rows), (3, 0, rows)]
-
-    def urow(i):
-        b, at, count = units[i]
-        return pl.multiple_of(slot(*order[b]) + at, hrows)
-
-    def core_copy(i):
-        at = pl.ds(urow(i), units[i][2])
-        return remote(part.at[at, pl.ds(its_col, cols)], r1.at[at, :], c_s.at[i], c_r.at[i], cpart)
 
     def finish(b):
         @pl.when(is_end)
@@ -437,23 +430,53 @@
                 dn_w, 0, 2 * width, width,
             )
 
-    def theirs(i):
-        slopes(urow(i), units[i][2])
-        back(urow(i), units[i][2], its_col)
-        core_copy(i).start()
-
-    def summed(i):
-        back(urow(i), units[i][2], my_col)
-        core_copy(i).wait_recv()
-        total(
-            (part, urow(i), my_col, cols),
-            [(part, urow(i), my_col, cols), (r1, urow(i), 0, cols)], units[i][2],
-        )
-
     here_row = slot(r, y)
 
     def plane_sums(pa):
         pb = cols - pa
+        pieces = [
+            (0, 0, hrows, 0, pa), (0, 0, hrows, pa, pb),
+            (0, hrows, hrows, 0, pa), (0, hrows, hrows, pa, pb),
+            (1, 0, rows, 0, cols), (2, 0, rows, 0, cols), (3, 0, rows, 0, cols),
+        ]
+
+        def place_of(i, col):
+            b, at, count, c0, n = pieces[i]
+            row = pl.multiple_of(slot(*order[b]) + at, hrows)
+            return row, count, pl.multiple_of(col + c0, 128), c0, n
+
+        def core_copy(i):
+            row, count, col, c0, n = place_of(i, its_col)
+            return remote(
+                part.at[pl.ds(row, count), pl.ds(col, n)],
+                r1.at[pl.ds(row, count), pl.ds(c0, n)], c_s.at[i], c_r.at[i], cpart,
+            )
+
+        def theirs(i):
+            row, count, col, c0, n = place_of(i, its_col)
+            if c0 == 0:
+                slopes(row, count)
+            back(row, count, col, n)
+            core_copy(i).start()
+
+        def summed(i):
+            row, count, col, c0, n = place_of(i, my_col)
+            back(row, count, col, n)
+            core_copy(i).wait_recv()
+            total((part, row, col, n), [(part, row, col, n), (r1, row, c0, n)], count)
+
+        def first_block():
+            for u in (0, 1):
+                theirs(2 * u)
+                theirs(2 * u + 1)
+                summed(2 * u)
+                x_copy(u).start()
+                summed(2 * u + 1)
+                y_copy(u).start()
+
+        def urow(u):
+            return pl.multiple_of(slot(*order[0]) + u * hrows, hrows)
+
         second_col = pl.multiple_of(my_col + pa, 128)
 
         def mine_a(row, count):
@@ -463,8 +486,9 @@
             return part.at[pl.ds(row, count), pl.ds(second_col, pb)]
 
         def x_copy(i):
-            if i == 3:
-                src, dst = s3b.at[:, pl.ds(0, pb)], rxb.at[:, pl.ds(0, pb)]
+            if i >= 3:
+                at = pl.ds((i - 3) * hrows, hrows)
+                src, dst = s3b.at[at, pl.ds(0, pb)], rxb.at[at, pl.ds(0, pb)]
             elif i == 2:
                 src, dst = mine_a(slot(*order[1]), rows), rxa.at[1, :, pl.ds(0, pa)]
             else:
@@ -489,7 +513,6 @@
                 (s3a, 0, 0, pa),
                 [(part, slot(r, 1 - y), my_col, pa), (rxa.at[0], 0, 0, pa)], rows,
             )
-            y_copy(4).start()
 
         def relay_b():
             for i in (0, 1):
@@ -524,8 +547,7 @@
 
         def final_b(i):
             at = i * hrows
-            if i == 0:
-                x_copy(3).wait_recv()
+            x_copy(3 + i).wait_recv()
             y_copy(2 + i).wait_recv()
             total(
                 (gi_out, at, second_col, pb),
@@ -537,15 +559,19 @@
             o_copy(1 + i, False).start()
 
         def settled():
+            for i in range(7):
+                core_copy(i).wait_send()
             for i in range(5):
                 y_copy(i).wait_send()
-            for i in range(4):
                 x_copy(i).wait_send()
             for i in range(3):
                 o_copy(i, True).wait_recv()
                 o_copy(i, False).wait_send()
 
-        return x_copy, y_copy, relay_a, relay_b, final_a, final_b, settled
+        return (
+            first_block, theirs, summed, x_copy, y_copy, relay_a, relay_b,
+            final_a, final_b, settled,
+        )
 
     def scaled(terms, rr, yy):
         at_col = gcol(rr, yy)
@@ -566,7 +592,10 @@
 
     @pl.when(is_end)
     def _():
-        x_copy, y_copy, relay_a, relay_b, final_a, final_b, settled = plane_sums(end_a)
+        (
+            first_block, theirs, summed, x_copy, y_copy, relay_a, relay_b,
+            final_a, final_b, settled,
+        ) = plane_sums(end_a)
         for i in range(line):
             g_block(jnp.where(lower, line - 1 - i, i))
             if i < line - 1:
@@ -590,26 +619,23 @@
             await_recv(up_dir, last, 1, 2)
         inputs_sent()
         finish(0)
-        theirs(0)
-        theirs(1)
-        for i in (0, 1):
-            summed(i)
-            x_copy(i).start()
-            y_copy(i).start()
+        first_block()
         finish(1)
-        theirs(2)
-        summed(2)
+        theirs(4)
+        summed(4)
         x_copy(2).start()
         finish(2)
-        theirs(3)
-        summed(3)
+        theirs(5)
+        summed(5)
         y_copy(2).start()
         finish(3)
-        theirs(4)
-        summed(4)
+        theirs(6)
+        summed(6)
         relay_a()
+        y_copy(4).start()
         y_copy(3).start()
         relay_b()
+        x_copy(4).start()
         h_copy(0).wait_recv()
         scaled([(g, pl.multiple_of(zrow + y * frows, frows), 0), (hl, 0, gcol(r, y))], r, y)
         final_a()
@@ -628,24 +654,22 @@
 
     @pl.when(jnp.logical_not(is_end))
     def _():
-        x_copy, y_copy, relay_a, relay_b, final_a, final_b, settled = plane_sums(mid_a)
+        (
+            first_block, theirs, summed, x_copy, y_copy, relay_a, relay_b,
+            final_a, final_b, settled,
+        ) = plane_sums(mid_a)
         inputs_sent()
         forward(1, dn_w, 2 * width, width, 3, 1)
-        theirs(0)
-        theirs(1)
-        for i in (0, 1):
-            summed(i)
-            x_copy(i).start()
-            y_copy(i).start()
+        first_block()
         g_block(jnp.where(lower, line - 1, 0))
         forward(1, dn_w, 2 * width, width, 1, 1)
-        theirs(2)
-        summed(2)
+        theirs(4)
+        summed(4)
         x_copy(2).start()
         line_step(1)
         forward(1, dn_w, 2 * width, width, 2, 1)
-        theirs(3)
-        summed(3)
+        theirs(5)
+        summed(5)
         y_copy(2).start()
         relay_a()
         relay_b()
@@ -653,9 +677,11 @@
             g_block(jnp.where(lower, line - 1 - i, i))
         for t in range(2, line - 1):
             line_step(t)
+        y_copy(4).start()
+        x_copy(4).start()
         forward(1, dn_w, 2 * width, width, 0, 1)
-        theirs(4)
-        summed(4)
+        theirs(6)
+        summed(6)
         up_copy(z, False).wait_recv()
         dn_copy(z, False).wait_recv()
         total(
@@ -712,8 +738,6 @@
             for sub in range(2):
                 await_send(True, d, sub, k)
                 await_send(False, d, sub, k)
-    for i in range(5):
-        core_copy(i).wait_send()
     for i in range(3):
         f_copy(i, False).wait_send()
     for zt in range(line):
@@ -764,7 +788,7 @@
             zsem, zsem, zsem, zsem,
             dma((3,)), dma((3,)),
             dma((8,)), dma((8,)), dma((8,)), dma((8,)), dma((5,)),
-            dma((5,)), dma((5,)), dma((4,)), dma((4,)), dma((5,)), dma((5,)),
+            dma((7,)), dma((7,)), dma((5,)), dma((5,)), dma((5,)), dma((5,)),
             dma((line,)), dma((line,)), dma((line,)), dma((line,)),
             dma((3,)), dma((3,)), dma((3,)), dma((3,)),
             dma((3,)), dma((3,)), dma((4,)), dma((4,)),

time: 154 us -> 154 us (level)
  no operation moved by 1% of the time
where the time goes in v7:
time: 154 us
  Pallas kernels  153 us (99%)
    pallas_call x1, Pallas kernels, fused(): pl.pallas_call(functools.partial(fused_kernel, line, grad_scale, end_a, m...  151 us

profile of v7, /device:TPU:0, one launch (start us, length us, event | category | flops | bytes accessed | tf_op | source)
XLA Modules:
  0.0 153.8 jit_solution(2194731379429625776)
XLA Ops:
  0.6 151.0 %fused_all.1 = (bf16[512,2048]{1,0:T(8,128)(2,1)S(1)}, f32[256,2048]{1,0:T(8,128)S(1)}) custom-call(bf16[256,2048]{1,0:T(8,128)(2,1)} %gate_w.1, bf16[256,2048]{1,0:T(8,128)(2,1)} %up_w.1, bf16[256,2048]{1,0:T(8,128)(2,1)} %down_w.1, bf16[512,2048]{1,0:T(8,128)(2,1)} %toks.1, bf16[512,2048]{1,0:T(8,128)(2,1)} %cots.1), custom_call_target="tpu_custom_call" | custom-call | tf_op jit(solution)/shard_map/fused_all/pallas_call | solution.py:765
  151.6 2.0 %place.1 = (bf16[512,2048]{1,0:T(8,128)(2,1)}, f32[256,2048]{1,0:T(8,128)}) custom-call(bf16[512,2048]{1,0:T(8,128)(2,1)S(1)} %get-tuple-element.4.a, f32[256,2048]{1,0:T(8,128)S(1)} %get-tuple-element.5.b), custom_call_target="tpu_custom_call" | custom-call | tf_op jit(solution)/shard_map/place/pallas_call | solution.py:816

commit v8 on v7

--- a/solution.py
+++ b/solution.py
@@ -368,31 +368,33 @@
         is_d = (z < line - 1) & (zd >= 0) & (zd < z)
         final = t == line - 2
 
-        @pl.when(is_u)
-        def _():
+        def add_u():
             up_copy(zt, False).wait_recv()
             total((u_in, row_u, 0, width), [(g, row_u, 0, width), (u_in, row_u, 0, width)], zrows)
 
-        @pl.when((is_u & (z < line - 2)) if final else is_u)
-        def _():
-            up_copy(zt, False).start()
-
-        @pl.when(is_d)
-        def _():
+        def add_d():
             dn_copy(zd, False).wait_recv()
             total((d_in, row_d, 0, width), [(g, row_d, 0, width), (d_in, row_d, 0, width)], zrows)
 
+        @pl.when((is_u & (z < line - 2)) if final else is_u)
+        def _():
+            add_u()
+            up_copy(zt, False).start()
+
         @pl.when((is_d & (z > 1)) if final else is_d)
         def _():
+            add_d()
             dn_copy(zd, False).start()
 
         if final:
             @pl.when(z == line - 2)
             def _():
+                add_u()
                 share(u_in, (line - 1) * zrows)
 
             @pl.when(z == 1)
             def _():
+                add_d()
                 share(d_in, 0)
 
     order = [(1 - r, 1 - y), (1 - r, y), (r, 1 - y), (r, y)]
@@ -466,13 +468,18 @@
             total((part, row, col, n), [(part, row, col, n), (r1, row, c0, n)], count)
 
         def first_block():
-            for u in (0, 1):
-                theirs(2 * u)
-                theirs(2 * u + 1)
-                summed(2 * u)
-                x_copy(u).start()
-                summed(2 * u + 1)
-                y_copy(u).start()
+            theirs(0)
+            theirs(1)
+            theirs(2)
+            summed(0)
+            x_copy(0).start()
+            summed(1)
+            y_copy(0).start()
+            theirs(3)
+            summed(2)
+            x_copy(1).start()
+            summed(3)
+            y_copy(1).start()
 
         def urow(u):
             return pl.multiple_of(slot(*order[0]) + u * hrows, hrows)
@@ -664,9 +671,9 @@
         g_block(jnp.where(lower, line - 1, 0))
         forward(1, dn_w, 2 * width, width, 1, 1)
         theirs(4)
+        line_step(1)
         summed(4)
         x_copy(2).start()
-        line_step(1)
         forward(1, dn_w, 2 * width, width, 2, 1)
         theirs(5)
         summed(5)
@@ -682,6 +689,15 @@
         forward(1, dn_w, 2 * width, width, 0, 1)
         theirs(6)
         summed(6)
+
+        @pl.when(next_to_end)
+        def _():
+            e_copy(0, True).wait_recv()
+            e_copy(2, False).start()
+            h_copy(1).start()
+            e_copy(1, True).wait_recv()
+            h_copy(2).start()
+
         up_copy(z, False).wait_recv()
         dn_copy(z, False).wait_recv()
         total(
@@ -691,15 +707,6 @@
         f_copy(0, False).start()
         y_copy(3).start()
         scaled([(gfin, pl.multiple_of(y * frows, frows), 0)], r, y)
-
-        @pl.when(next_to_end)
-        def _():
-            e_copy(0, True).wait_recv()
-            e_copy(2, False).start()
-            h_copy(1).start()
-            e_copy(1, True).wait_recv()
-            h_copy(2).start()
-
         f_copy(1, False).start()
         final_a()
         final_b(0)

time: 154 us -> 153 us (level)
  Pallas kernels: 153 us -> 151 us
    pallas_call x1, Pallas kernels: 151 us -> 149 us  [fused(): pl.pallas_call(functools.partial(fused_kernel, line, grad_scale, end_a, m...]
where the time goes in v8:
time: 153 us; the launch traced here: 152 us
  Pallas kernels  151 us (99%)
    pallas_call x1, Pallas kernels, fused(): pl.pallas_call(functools.partial(fused_kernel, line, grad_scale, end_a, m...  149 us

profile of v8, /device:TPU:0, one launch (start us, length us, event | category | flops | bytes accessed | tf_op | source)
XLA Modules:
  0.0 151.9 jit_solution(9524902750701862336)
XLA Ops:
  0.6 149.1 %fused_all.1 = (bf16[512,2048]{1,0:T(8,128)(2,1)S(1)}, f32[256,2048]{1,0:T(8,128)S(1)}) custom-call(bf16[256,2048]{1,0:T(8,128)(2,1)} %gate_w.1, bf16[256,2048]{1,0:T(8,128)(2,1)} %up_w.1, bf16[256,2048]{1,0:T(8,128)(2,1)} %down_w.1, bf16[512,2048]{1,0:T(8,128)(2,1)} %toks.1, bf16[512,2048]{1,0:T(8,128)(2,1)} %cots.1), custom_call_target="tpu_custom_call" | custom-call | tf_op jit(solution)/shard_map/fused_all/pallas_call | solution.py:772
  149.8 2.0 %place.1 = (bf16[512,2048]{1,0:T(8,128)(2,1)}, f32[256,2048]{1,0:T(8,128)}) custom-call(bf16[512,2048]{1,0:T(8,128)(2,1)S(1)} %get-tuple-element.4.a, f32[256,2048]{1,0:T(8,128)S(1)} %get-tuple-element.5.b), custom_call_target="tpu_custom_call" | custom-call | tf_op jit(solution)/shard_map/place/pallas_call | solution.py:823

commit v9 on v8

--- a/solution.py
+++ b/solution.py
@@ -14,7 +14,7 @@
 def fused_kernel(
     line, grad_scale, end_a, mid_a, gate_w, up_w, down_w, toks, cots, gi_out, gd_out,
     x, gu, dn_w, acc, hid, ggu, r1, rxa, rxb, rya, ryb, s3a, s3b, g, u_in, d_in, gfin, gl, hl,
-    up_s, up_r, dn_s, dn_r, wy_s, wy_r, tok_s, tok_r, d2d_s, d2d_r, loc,
+    z_s, up_r, dn_r, wy_s, wy_r, tok_s, tok_r, d2d_s, d2d_r, loc,
     c_s, c_r, x_s, x_r, yy_s, yy_r, u_s, u_r, d_s, d_r, f_s, f_r, o_s, o_r, e_s, e_r, h_s, h_r,
 ):
     r = lax.axis_index("rep")
@@ -69,8 +69,8 @@
     def zcopy(up_dir, d, sub, k, zz):
         yy = y if sub == 0 else 1 - y
         src = own(k, y) if (d == 0 and sub == 0) else wblk(k, zz, yy)
-        s, q, dev = (up_s, up_r, up) if up_dir else (dn_s, dn_r, dn)
-        return remote(src, wblk(k, zz, yy), s.at[d, sub, k], q.at[d, sub, k], dev)
+        q, dev = (up_r, up) if up_dir else (dn_r, dn)
+        return remote(src, wblk(k, zz, yy), z_s, q.at[d, sub, k], dev)
 
     def pred_send(up_dir, d):
         return (has_up & (z - d >= 0)) if up_dir else (has_dn & (z + d <= line - 1))
@@ -82,11 +82,6 @@
         @pl.when(pred_send(up_dir, d))
         def _():
             zcopy(up_dir, d, sub, k, src_z(up_dir, d)).start()
-
-    def await_send(up_dir, d, sub, k):
-        @pl.when(pred_send(up_dir, d))
-        def _():
-            zcopy(up_dir, d, sub, k, src_z(up_dir, d)).wait_send()
 
     def await_recv(up_dir, d, sub, k):
         ok = (z - d - 1 >= 0) if up_dir else (z + d + 1 <= line - 1)
@@ -292,10 +287,6 @@
         acc[at, pl.ds(0, width)] = up_val * sig * (1.0 + gate * (1.0 - sig))
         acc[at, pl.ds(width, width)] = active
 
-    for i in (2, 6, 7):
-        event(i)
-    for i in (1, 2, 4, 6, 7):
-        dcopy(i, 1 - core).wait_recv()
 
     zrow = pl.multiple_of(z * zrows, zrows)
     lower = z < line // 2
@@ -603,6 +594,10 @@
             first_block, theirs, summed, x_copy, y_copy, relay_a, relay_b,
             final_a, final_b, settled,
         ) = plane_sums(end_a)
+        for i in (2, 6, 7):
+            event(i)
+        for i in (1, 2, 4, 6, 7):
+            dcopy(i, 1 - core).wait_recv()
         for i in range(line):
             g_block(jnp.where(lower, line - 1 - i, i))
             if i < line - 1:
@@ -665,30 +660,39 @@
             first_block, theirs, summed, x_copy, y_copy, relay_a, relay_b,
             final_a, final_b, settled,
         ) = plane_sums(mid_a)
+        event(2)
         inputs_sent()
+        for i in (1, 2):
+            dcopy(i, 1 - core).wait_recv()
+        forward(1, dn_w, 2 * width, width, 1, 1)
+        theirs(4)
+        summed(4)
+        x_copy(2).start()
+        event(6)
+        dcopy(4, 1 - core).wait_recv()
+        forward(1, dn_w, 2 * width, width, 2, 1)
+        theirs(5)
+        event(7)
+        summed(5)
+        y_copy(2).start()
+        y_copy(3).start()
+        for i in (6, 7):
+            dcopy(i, 1 - core).wait_recv()
         forward(1, dn_w, 2 * width, width, 3, 1)
         first_block()
         g_block(jnp.where(lower, line - 1, 0))
-        forward(1, dn_w, 2 * width, width, 1, 1)
-        theirs(4)
         line_step(1)
-        summed(4)
-        x_copy(2).start()
-        forward(1, dn_w, 2 * width, width, 2, 1)
-        theirs(5)
-        summed(5)
-        y_copy(2).start()
+        for i in range(1, line):
+            g_block(jnp.where(lower, line - 1 - i, i))
+        forward(1, dn_w, 2 * width, width, 0, 1)
+        theirs(6)
+        summed(6)
         relay_a()
         relay_b()
-        for i in range(1, line):
-            g_block(jnp.where(lower, line - 1 - i, i))
         for t in range(2, line - 1):
             line_step(t)
         y_copy(4).start()
         x_copy(4).start()
-        forward(1, dn_w, 2 * width, width, 0, 1)
-        theirs(6)
-        summed(6)
 
         @pl.when(next_to_end)
         def _():
@@ -705,7 +709,6 @@
             [(g, zrow, 0, width), (u_in, zrow, 0, width), (d_in, zrow, 0, width)], zrows,
         )
         f_copy(0, False).start()
-        y_copy(3).start()
         scaled([(gfin, pl.multiple_of(y * frows, frows), 0)], r, y)
         f_copy(1, False).start()
         final_a()
@@ -741,10 +744,14 @@
             tcopy(i, False).wait_send()
     for k in range(3):
         to_y(k).wait_send()
-        for d in range(line - 1):
-            for sub in range(2):
-                await_send(True, d, sub, k)
-                await_send(False, d, sub, k)
+
+    unit = wrows * width // (2 * x.shape[2])
+    for count, here in ((6, is_end), (6 * (line + 1), jnp.logical_not(is_end))):
+        @pl.when(here)
+        def _(count=count):
+            view = x.at[:, pl.ds(0, count * unit), :]
+            pltpu.make_async_copy(view, view, z_s).wait()
+
     for i in range(3):
         f_copy(i, False).wait_send()
     for zt in range(line):
@@ -792,7 +799,7 @@
             pltpu.VMEM((2 * wrows, width), kind),
             pltpu.VMEM((wrows, 4 * width), kind),
             pltpu.VMEM((wrows, 4 * width), kind),
-            zsem, zsem, zsem, zsem,
+            dma, zsem, zsem,
             dma((3,)), dma((3,)),
             dma((8,)), dma((8,)), dma((8,)), dma((8,)), dma((5,)),
             dma((7,)), dma((7,)), dma((5,)), dma((5,)), dma((5,)), dma((5,)),

time: 153 us -> 162 us (1.059)
  Pallas kernels: 151 us -> 159 us
    pallas_call x1, Pallas kernels: 149 us -> 157 us  [fused(): pl.pallas_call(functools.partial(fused_kernel, line, grad_scale, end_a, m...]
where the time goes in v9:
time: 162 us; the launch traced here: 160 us
  Pallas kernels  159 us (98%)
    pallas_call x1, Pallas kernels, fused(): pl.pallas_call(functools.partial(fused_kernel, line, grad_scale, end_a, m...  157 us

profile of v9, /device:TPU:0, one launch (start us, length us, event | category | flops | bytes accessed | tf_op | source)
XLA Modules:
  0.0 160.3 jit_solution(9234309774849886758)
XLA Ops:
  0.6 157.5 %fused_all.1 = (bf16[512,2048]{1,0:T(8,128)(2,1)S(1)}, f32[256,2048]{1,0:T(8,128)S(1)}) custom-call(bf16[256,2048]{1,0:T(8,128)(2,1)} %gate_w.1, bf16[256,2048]{1,0:T(8,128)(2,1)} %up_w.1, bf16[256,2048]{1,0:T(8,128)(2,1)} %down_w.1, bf16[512,2048]{1,0:T(8,128)(2,1)} %toks.1, bf16[512,2048]{1,0:T(8,128)(2,1)} %cots.1), custom_call_target="tpu_custom_call" | custom-call | tf_op jit(solution)/shard_map/fused_all/pallas_call | solution.py:779
  158.1 2.0 %place.1 = (bf16[512,2048]{1,0:T(8,128)(2,1)}, f32[256,2048]{1,0:T(8,128)}) custom-call(bf16[512,2048]{1,0:T(8,128)(2,1)S(1)} %get-tuple-element.4.a, f32[256,2048]{1,0:T(8,128)S(1)} %get-tuple-element.5.b), custom_call_target="tpu_custom_call" | custom-call | tf_op jit(solution)/shard_map/place/pallas_call | solution.py:830

commit v10 on v9

--- a/solution.py
+++ b/solution.py
@@ -674,12 +674,12 @@
         theirs(5)
         event(7)
         summed(5)
-        y_copy(2).start()
-        y_copy(3).start()
         for i in (6, 7):
             dcopy(i, 1 - core).wait_recv()
         forward(1, dn_w, 2 * width, width, 3, 1)
         first_block()
+        y_copy(2).start()
+        y_copy(3).start()
         g_block(jnp.where(lower, line - 1, 0))
         line_step(1)
         for i in range(1, line):
@@ -774,7 +774,7 @@
     zsem = dma((line - 1, 2, 3))
     anyspec = pl.BlockSpec(memory_space=pl.ANY)
     whole = pltpu.VMEM((depth, width), kind)
-    end_a, mid_a = cols // 2, cols * 3 // 8 // 128 * 128
+    end_a, mid_a = cols // 2, cols // 2
     most_b = cols - mid_a
     return pl.pallas_call(
         functools.partial(fused_kernel, line, grad_scale, end_a, mid_a),

time: 162 us -> 153 us (0.944)
  Pallas kernels: 159 us -> 151 us
    pallas_call x1, Pallas kernels: 157 us -> 149 us  [fused(): pl.pallas_call(functools.partial(fused_kernel, line, grad_scale, end_a, m...]
where the time goes in v10:
time: 153 us; the launch traced here: 152 us
  Pallas kernels  151 us (99%)
    pallas_call x1, Pallas kernels, fused(): pl.pallas_call(functools.partial(fused_kernel, line, grad_scale, end_a, m...  149 us

profile of v10, /device:TPU:0, one launch (start us, length us, event | category | flops | bytes accessed | tf_op | source)
XLA Modules:
  0.0 151.6 jit_solution(1557162138913166687)
XLA Ops:
  0.6 148.8 %fused_all.1 = (bf16[512,2048]{1,0:T(8,128)(2,1)S(1)}, f32[256,2048]{1,0:T(8,128)S(1)}) custom-call(bf16[256,2048]{1,0:T(8,128)(2,1)} %gate_w.1, bf16[256,2048]{1,0:T(8,128)(2,1)} %up_w.1, bf16[256,2048]{1,0:T(8,128)(2,1)} %down_w.1, bf16[512,2048]{1,0:T(8,128)(2,1)} %toks.1, bf16[512,2048]{1,0:T(8,128)(2,1)} %cots.1), custom_call_target="tpu_custom_call" | custom-call | tf_op jit(solution)/shard_map/fused_all/pallas_call | solution.py:779
  149.4 2.0 %place.1 = (bf16[512,2048]{1,0:T(8,128)(2,1)}, f32[256,2048]{1,0:T(8,128)}) custom-call(bf16[512,2048]{1,0:T(8,128)(2,1)S(1)} %get-tuple-element.4.a, f32[256,2048]{1,0:T(8,128)S(1)} %get-tuple-element.5.b), custom_call_target="tpu_custom_call" | custom-call | tf_op jit(solution)/shard_map/place/pallas_call | solution.py:830
